TPU v7x, 128 devices: a whole 4x4x4 slice. The times are simulated.
128 devices in a mesh: fs: 16 (over z, x), tp: 8 (over y, core).
Axes of the slice: x: 4, y: 4, z: 4, core: 2. Of those that a mesh axis runs over, the one named last changes fastest.
Arguments:
- h_saved: bfloat16 [32768, 2048], P('fs'), may hold values from -6 to 6
- conv_cotan: bfloat16 [32768, 2560], P('fs', 'tp'), may hold values from -64 to 64
- lru_out: bfloat16 [32768, 2560], P('fs', 'tp'), may hold values from -64 to 64
- out_cotan: bfloat16 [32768, 2048], P('fs'), may hold values from -6 to 6
- basis_in: bfloat16 [2048, 256], P('fs'), may hold values from -1.41421356 to 1.41421356
- basis_out: bfloat16 [2048, 256], P('fs'), may hold values from -1.41421356 to 1.41421356
- weight_in: float32 [2048, 2560], P('fs', 'tp'), may hold values from -0.125 to 0.125
- weight_out: float32 [2560, 2048], P('tp', 'fs'), may hold values from -0.125 to 0.125
- first_in: float32 [256, 2560], P('fs', 'tp'), may hold values from -6 to 6
- second_in: float32 [256, 2560], P('fs', 'tp'), may hold values from 0.05 to 2
- first_out: float32 [256, 2560], P('fs', 'tp'), may hold values from -6 to 6
- second_out: float32 [256, 2560], P('fs', 'tp'), may hold values from 0.05 to 2
Outputs:
- step_in: float32 [2048, 2560], P('fs', 'tp')
- new_weight_in: float32 [2048, 2560], P('fs', 'tp')
- copy_in: bfloat16 [2048, 2560], P(None, 'tp')
- new_first_in: float32 [256, 2560], P('fs', 'tp')
- new_second_in: float32 [256, 2560], P('fs', 'tp')
- step_out: float32 [2560, 2048], P('tp', 'fs')
- new_weight_out: float32 [2560, 2048], P('tp', 'fs')
- copy_out: bfloat16 [2560, 2048], P('tp')
- new_first_out: float32 [256, 2560], P('fs', 'tp')
- new_second_out: float32 [256, 2560], P('fs', 'tp')
All inputs are finite; a program needn't handle non-finite values.
Results may differ from a plain program's by a relative error of at most 0.0046.
Values may be sent and summed in bfloat16 or wider, within the bound.
No kernel may reach another device: no remote copies, remote signals or barrier semaphores. Data moves between devices by JAX's collectives and lax.ppermute only.
A program may use at most 128 MiB of HBM per device.

v0:
```python
import math

import jax
import jax.numpy as jnp
from jax import lax
from jax.experimental import pallas as pl
from jax.experimental.pallas import tpu as pltpu
from jax.sharding import Mesh
from jax.sharding import PartitionSpec as P

D_RNN = 2560
RANK = 256
FS = ("fs_0", "fs_1")
TP = ("tp_0", "tp_1")
EVERY = ("fs_0", "fs_1", "tp_0", "tp_1")
BF16 = jnp.bfloat16
F32 = jnp.float32

W = 320
ROWS = 16
PEERS = 16
SIDE = 4

LIMIT = pltpu.CompilerParams(vmem_limit_bytes=20 << 20)
VMEM = pl.BlockSpec(memory_space=pltpu.VMEM)
SMEM = pl.BlockSpec(memory_space=pltpu.SMEM)


def swapped(array):
    return lax.ppermute(array, "tp_1", [(0, 1), (1, 0)])


def shifted(array, axis, by):
    return lax.ppermute(array, axis, [(i, (i + by) % SIDE) for i in range(SIDE)])


def sent_to_all(array, axis):
    copies = jnp.broadcast_to(array, (lax.axis_size(axis), *array.shape))
    return lax.all_to_all(copies, axis, split_axis=0, concat_axis=0, tiled=True)


def contract(a, b, dims):
    return lax.dot_general(a, b, (dims, ((), ())), preferred_element_type=F32)


def pack_kernel(w_in, w_out, out):
    out[0:W, :] = w_in[...].astype(BF16)
    out[W : 2 * W, :] = w_out[...].astype(BF16)


def pack(*args):
    return pl.pallas_call(
        pack_kernel,
        out_shape=jax.ShapeDtypeStruct((2 * W, 128), BF16),
        in_specs=[VMEM] * 2,
        out_specs=VMEM,
        name="pack",
        compiler_params=LIMIT,
        cost_estimate=pl.CostEstimate(flops=10**6, bytes_accessed=500_000, transcendentals=0),
    )(*args)


def grads_kernel(where, conv, lru, h, o, keep, send):
    takes_in = where[0] == 0
    g_in = jnp.dot(conv[...], h[...], preferred_element_type=F32)
    g_out = jnp.dot(lru[...], o[...], preferred_element_type=F32)
    keep[...] = jnp.where(takes_in, g_in, g_out).astype(BF16)
    send[...] = jnp.where(takes_in, g_out, g_in).astype(BF16)


def grads(where, conv, lru, h, o):
    tile = 256
    wide = pl.BlockSpec((W, 2048), lambda i: (0, 0))
    tall = pl.BlockSpec((2048, tile), lambda i: (0, i))
    out = pl.BlockSpec((W, tile), lambda i: (0, i))
    return pl.pallas_call(
        grads_kernel,
        grid=(2048 // tile,),
        in_specs=[SMEM, wide, wide, tall, tall],
        out_specs=(out, out),
        out_shape=(jax.ShapeDtypeStruct((W, 2048), BF16),) * 2,
        name="grads",
        compiler_params=pltpu.CompilerParams(vmem_limit_bytes=57 << 20),
        cost_estimate=pl.CostEstimate(
            flops=4 * 2048 * 2048 * W, bytes_accessed=22_000_000, transcendentals=0
        ),
    )(where, conv, lru, h, o)


def project_kernel(kept, came, basis, out, total):
    n = pl.program_id(0)
    mine = jnp.dot(kept[...], basis[...], preferred_element_type=F32)
    other = jnp.dot(came[...], basis[...], preferred_element_type=F32)

    @pl.when(n == 0)
    def _():
        total[0:W] = mine
        total[W:] = other

    @pl.when(n > 0)
    def _():
        total[0:W] += mine
        total[W:] += other

    @pl.when(n == pl.num_programs(0) - 1)
    def _():
        out[...] = total[...].T.astype(BF16)


def project(kept, came, basis):
    tile = 512
    wide = pl.BlockSpec((W, tile), lambda i: (0, i))
    return pl.pallas_call(
        project_kernel,
        grid=(2048 // tile,),
        in_specs=[wide, wide, pl.BlockSpec((tile, RANK), lambda i: (i, 0))],
        out_specs=pl.BlockSpec((RANK, 2 * W), lambda i: (0, 0)),
        out_shape=jax.ShapeDtypeStruct((RANK, 2 * W), BF16),
        scratch_shapes=[pltpu.VMEM((2 * W, RANK), F32)],
        name="project",
        compiler_params=LIMIT,
        cost_estimate=pl.CostEstimate(
            flops=4 * 2048 * RANK * W, bytes_accessed=4_000_000, transcendentals=0
        ),
    )(kept, came, basis)


def moments(proj, factor, first, second):
    scaled = factor * proj
    first_new = 0.8 * first + 0.2 * scaled
    second_new = 0.9 * second + 0.1 * scaled * scaled
    direction = (first_new / (jnp.sqrt(second_new) + 1e-08)).astype(BF16)
    return (first_new, second_new, direction)


ORDER_Z = (0, 1, 3, 2)
ORDER_X = (0, 1, 3, 2)


def final_kernel(
    where,
    full,
    b_in,
    b_out,
    w_in,
    w_out,
    basis_own,
    basis_other,
    old_0,
    old_1,
    old_3,
    old_2a,
    old_2b,
    step_in,
    new_in,
    copy_in,
    step_out,
    new_out,
    copy_out,
    turned,
    s_in,
    s_out,
):
    takes_in = where[0] == 0
    n = pl.program_id(0)

    @pl.when(n == 0)
    def _():
        turned[...] = full[...].astype(F32).T.astype(BF16)
        own_in = contract(turned[0:W], b_in[...], ((1,), (1,)))
        own_out = contract(turned[W:], b_out[...], ((1,), (1,)))
        step_in[...] = own_in
        step_out[...] = own_out
        new_in[...] = w_in[...] - 0.02 * own_in
        new_out[...] = w_out[...] - 0.02 * own_out

    own = basis_own[...]
    other = basis_other[...]
    s_in[...] = contract(turned[0:W], jnp.where(takes_in, own, other), ((1,), (1,)))
    s_out[...] = contract(turned[W:], jnp.where(takes_in, other, own), ((1,), (1,)))

    def write(block, k):
        at = lax.rem(where[1] + ORDER_X[k], SIDE)
        cols = pl.ds(pl.multiple_of(at * 128, 128), 128)
        block = block.astype(F32)
        copy_in[:, cols] = (block[0:W] - 0.02 * s_in[:, cols]).astype(BF16)
        copy_out[:, cols] = (block[W:] - 0.02 * s_out[:, cols]).astype(BF16)

    for step, old in enumerate((old_0, old_1, old_3)):

        @pl.when(n == step)
        def _():
            for k in range(SIDE):
                write(old[k], k)

    @pl.when(n == 3)
    def _():
        for k in range(SIDE):
            write(old_2a[k] if k < 2 else old_2b[k - 2], k)


def final(where, full, bases, weights, own, other, old):
    shape = jax.ShapeDtypeStruct

    def whole(s):
        return pl.BlockSpec(s, lambda i, where: (0,) * len(s))

    tall = whole((W, 128))
    tile = pl.BlockSpec((512, RANK), lambda i, where: (where[2 + i], 0))
    copy = pl.BlockSpec((W, 512), lambda i, where: (0, where[2 + i]))
    return pl.pallas_call(
        final_kernel,
        grid_spec=pltpu.PrefetchScalarGridSpec(
            num_scalar_prefetch=1,
            grid=(SIDE,),
            in_specs=[
                whole((RANK, 2 * W)),
                whole((128, RANK)),
                whole((128, RANK)),
                tall,
                tall,
                tile,
                tile,
                *[whole((SIDE, 2 * W, 128))] * 3,
                *[whole((2, 2 * W, 128))] * 2,
            ],
            out_specs=(tall, tall, copy, tall, tall, copy),
            scratch_shapes=[
                pltpu.VMEM((2 * W, RANK), BF16),
                pltpu.VMEM((W, 512), F32),
                pltpu.VMEM((W, 512), F32),
            ],
        ),
        out_shape=(
            shape((W, 128), F32),
            shape((W, 128), F32),
            shape((W, 2048), BF16),
            shape((W, 128), F32),
            shape((W, 128), F32),
            shape((W, 2048), BF16),
        ),
        name="final",
        compiler_params=LIMIT,
        cost_estimate=pl.CostEstimate(
            flops=700_000_000, bytes_accessed=10_000_000, transcendentals=0
        ),
    )(where, full, *bases, *weights, own, other, *old)


def shards(
    h_saved,
    conv_cotan,
    lru_out,
    out_cotan,
    basis_in,
    basis_out,
    weight_in,
    weight_out,
    first_in,
    second_in,
    first_out,
    second_out,
):
    core = lax.axis_index("tp_1").astype(jnp.int32)
    at_z = lax.axis_index("fs_0").astype(jnp.int32)
    at_x = lax.axis_index("fs_1").astype(jnp.int32)
    takes_in = core == 0
    where = jnp.stack([core, at_x, *((at_z + d) & (SIDE - 1) for d in ORDER_Z)])

    mine = jnp.where(takes_in, basis_in, basis_out)
    basis_own = sent_to_all(mine, FS).reshape(-1, RANK)
    basis_other = swapped(basis_own)

    packed = pack(weight_in.T, weight_out)
    pieces = [packed]
    for d in ORDER_X[1:]:
        pieces.append(shifted(packed, "fs_1", -d))
    bundle = lax.optimization_barrier(jnp.stack(pieces))
    bundle_1 = shifted(bundle, "fs_0", -1)
    bundle_3 = shifted(bundle, "fs_0", -3)
    bundle_2a = shifted(bundle_1[:2], "fs_0", -1)
    bundle_2b = shifted(bundle_3[2:], "fs_0", -3)
    old = (bundle, bundle_1, bundle_3, bundle_2a, bundle_2b)

    kept, given = grads(where, conv_cotan.T, lru_out.T, h_saved, out_cotan)
    came = swapped(given)
    part = project(kept, came, basis_own)
    arrived = lax.all_to_all(
        part.reshape(PEERS, ROWS, 2 * W), FS, split_axis=0, concat_axis=0, tiled=True
    )
    proj = arrived.astype(F32).sum(axis=0)
    partial_total = jnp.broadcast_to(jnp.sum(proj * proj), (1, 128))
    total = jnp.sum(sent_to_all(partial_total, EVERY)[:, 0, 0])
    proj_own = proj[:, :W]
    proj_other = swapped(proj[:, W:])
    proj_in = jnp.where(takes_in, proj_own, proj_other)
    proj_out = jnp.where(takes_in, proj_other, proj_own)
    factor = math.sqrt(2.0 * RANK * D_RNN) * lax.rsqrt(total + 1e-06)
    first_a, second_a, dir_in = moments(proj_in, factor, first_in, second_in)
    first_b, second_b, dir_out = moments(proj_out, factor, first_out, second_out)
    full = sent_to_all(jnp.concatenate((dir_in, dir_out), axis=1), FS).reshape(RANK, 2 * W)
    step_in, new_in, copy_in, step_out, new_out, copy_out = final(
        where, full, (basis_in, basis_out), (weight_in.T, weight_out), basis_own, basis_other, old
    )
    return (
        step_in.T,
        new_in.T,
        copy_in.T,
        first_a,
        second_a,
        step_out,
        new_out,
        copy_out,
        first_b,
        second_b,
    )


def solution(mesh):
    finer = Mesh(mesh.devices.reshape(4, 4, 4, 2), EVERY)
    placed = (
        P(FS, None),
        P(FS, TP),
        P(FS, TP),
        P(FS, None),
        P(FS, None),
        P(FS, None),
        P(FS, TP),
        P(TP, FS),
        P(FS, TP),
        P(FS, TP),
        P(FS, TP),
        P(FS, TP),
    )
    return jax.shard_map(
        shards,
        mesh=finer,
        in_specs=placed,
        out_specs=(
            P(FS, TP),
            P(FS, TP),
            P(None, TP),
            P(FS, TP),
            P(FS, TP),
            P(TP, FS),
            P(TP, FS),
            P(TP, None),
            P(FS, TP),
            P(FS, TP),
        ),
        check_vma=False,
    )
```

profile of v0, /device:TPU:0, one launch (start us, length us, event | category | flops | bytes accessed | tf_op | source)
XLA Modules:
  0.0 113.1 jit_solution(7277883025630418802)
XLA Ops:
  0.7 0.6 stack.42.where
  1.3 0.0 copy-start.4
  1.3 0.0 copy-start.6
  1.3 13.0 %grads.1 = (bf16[320,2048]{1,0:T(8,128)(2,1)}, bf16[320,2048]{1,0:T(8,128)(2,1)}) custom-call(s32[6]{0:T(128)} %stack.42.where, bf16[320,2048]{1,0:T(8,128)(2,1)} %bitcast.29, bf16[320,2048]{1,0:T(8,128)(2,1)} %bitcast.30, bf16[2048,2048]{1,0:T(8,128)(2,1)} %h.1, bf16[2048,2048]{1,0:T(8,128)(2,1)} %o.1), custom_call_target="tpu_custom_call" | custom-call | flops 5368709120 | bytes 22000000 | tf_op jit(solution)/shard_map/grads/pallas_call | solution.py:76
  14.2 0.0 collective-permute-start
  14.3 0.0 copy-done.4
  14.3 0.0 copy-done.6
  14.3 1.1 broadcast_in_dim.6
  15.4 0.0 copy-start.1
  15.4 0.0 copy-start.2
  15.4 8.1 %all-to-all-start = ((bf16[16,128,256]{2,1,0:T(8,128)(2,1)}), bf16[16,128,256]{2,1,0:T(8,128)(2,1)S(1)}, u32[]{:S(2)}, u32[]{:S(2)}) async-start(bf16[16,128,256]{2,1,0:T(8,128)(2,1)} %broadcast_in_dim.6), calls=%async_computation | async-start | bytes 2097152 | tf_op jit(solution)/shard_map/all_to_all | solution.py:39
  23.5 0.0 copy-done.1
  23.5 0.0 copy-done.2
  23.5 3.2 %collective-permute-start.3 = (bf16[640,128]{1,0:T(8,128)(2,1)S(1)}, bf16[640,128]{1,0:T(8,128)(2,1)S(1)}, u32[]{:S(2)}, u32[]{:S(2)}) collective-permute-start(bf16[640,128]{1,0:T(8,128)(2,1)S(1)} %pack.1), channel_id=1, source_target_pairs={{0,24},{8,0},{16,8},{24,16},{1,25},{9,1},{17,9},{25,17},{2,26},{10... | collective-permute-start | bytes 491528 | tf_op jit(solution)/shard_map/ppermute | solution.py:34
  26.7 0.0 collective-permute-start.4
  26.7 2.3 %collective-permute-start.5 = (bf16[640,128]{1,0:T(8,128)(2,1)S(1)}, bf16[640,128]{1,0:T(8,128)(2,1)S(1)}, u32[]{:S(2)}, u32[]{:S(2)}) collective-permute-start(bf16[640,128]{1,0:T(8,128)(2,1)S(1)} %pack.1), channel_id=1, source_target_pairs={{0,16},{8,24},{16,0},{24,8},{1,17},{9,25},{17,1},{25,9},{2,18},{10... | collective-permute-start | bytes 491528 | tf_op jit(solution)/shard_map/ppermute | solution.py:34
  29.1 13.0 %collective-permute-done.3 = bf16[640,128]{1,0:T(8,128)(2,1)S(1)} collective-permute-done((bf16[640,128]{1,0:T(8,128)(2,1)S(1)}, bf16[640,128]{1,0:T(8,128)(2,1)S(1)}, u32[]{:S(2)}, u32[]{:S(2)}) %collective-permute-start.3) | collective-permute-done | bytes 163872 | tf_op jit(solution)/shard_map/ppermute | solution.py:34
  42.0 0.3 collective-permute-done.4
  42.4 4.7 %collective-permute-done.5 = bf16[640,128]{1,0:T(8,128)(2,1)S(1)} collective-permute-done((bf16[640,128]{1,0:T(8,128)(2,1)S(1)}, bf16[640,128]{1,0:T(8,128)(2,1)S(1)}, u32[]{:S(2)}, u32[]{:S(2)}) %collective-permute-start.5) | collective-permute-done | bytes 163872 | tf_op jit(solution)/shard_map/ppermute | solution.py:34
  47.0 0.1 pad_maximum_fusion.old_0
  47.1 2.4 %collective-permute-start.6 = (bf16[4,640,128]{2,1,0:T(8,128)(2,1)S(1)}, bf16[4,640,128]{2,1,0:T(8,128)(2,1)S(1)}, u32[]{:S(2)}, u32[]{:S(2)}) collective-permute-start(bf16[4,640,128]{2,1,0:T(8,128)(2,1)S(1)} %pad_maximum_fusion.old_0), channel_id=1, source_target_pairs={{0,96},{32,0},{64,32},{96,64},{1,97},{33,1},{65,33},{97,65},{2,98}... | collective-permute-start | bytes 1966088 | tf_op jit(solution)/shard_map/ppermute | solution.py:34
  49.5 0.0 collective-permute-start.7
  49.5 0.0 all-to-all-done
  49.5 0.0 collective-permute-done.came
  49.5 0.0 copy-start
  49.5 1.3 %copy-done = bf16[320,2048]{1,0:T(8,128)(2,1)S(1)} copy-done((bf16[320,2048]{1,0:T(8,128)(2,1)S(1)}, bf16[320,2048]{1,0:T(8,128)(2,1)}, u32[]{:S(2)}) %copy-start) | copy-done | bytes 1310744
  50.8 4.1 %project.1 = bf16[256,640]{1,0:T(8,128)(2,1)} custom-call(bf16[320,2048]{1,0:T(8,128)(2,1)S(1)} %copy-done, bf16[320,2048]{1,0:T(8,128)(2,1)} %collective-permute-done.came, bf16[2048,256]{1,0:T(8,128)(2,1)S(1)} %bitcast.19), custom_call_target="tpu_custom_call" | custom-call | flops 671088640 | bytes 4000000 | tf_op jit(solution)/shard_map/project/pallas_call | solution.py:113
  55.0 5.2 %all-to-all-start.1 = ((bf16[16,16,640]{2,1,0:T(8,128)(2,1)}), bf16[16,16,640]{2,1,0:T(8,128)(2,1)S(1)}, u32[]{:S(2)}, u32[]{:S(2)}) async-start(bf16[16,16,640]{2,1,0:T(8,128)(2,1)} %bitcast.9), calls=%async_computation.1 | async-start | bytes 655360 | tf_op jit(solution)/shard_map/all_to_all | solution.py:288
  60.1 0.1 collective-permute-start.2
  60.2 9.7 %all-to-all-done.1 = bf16[16,16,640]{2,1,0:T(8,128)(2,1)S(1)} async-done(((bf16[16,16,640]{2,1,0:T(8,128)(2,1)}), bf16[16,16,640]{2,1,0:T(8,128)(2,1)S(1)}, u32[]{:S(2)}, u32[]{:S(2)}) %all-to-all-start.1) | async-done | bytes 327712 | tf_op jit(solution)/shard_map/all_to_all | solution.py:288
  69.9 0.1 convert_reduce_fusion
  70.0 0.6 multiply_reduce_fusion
  70.6 1.3 %broadcast_in_dim_broadcast_in_dim.3 = f32[128,1,128]{2,1,0:T(1,128)} broadcast(f32[]{:T(128)} %multiply_reduce_fusion), dimensions={} | broadcast | bytes 65540 | tf_op jit(solution)/shard_map/broadcast_in_dim;broadcast_in_dim | solution.py:38
  71.9 6.4 %all-to-all-start.2 = ((f32[128,1,128]{2,1,0:T(1,128)}), f32[128,1,128]{2,1,0:T(1,128)S(1)}, u32[]{:S(2)}, u32[]{:S(2)}) async-start(f32[128,1,128]{2,1,0:T(1,128)} %broadcast_in_dim_broadcast_in_dim.3), calls=%async_computation.2 | async-start | bytes 131072 | tf_op jit(solution)/shard_map/all_to_all | solution.py:39
  78.3 0.0 copy-start.8
  78.3 0.0 collective-permute-done.6.old_1
  78.3 0.7 slice.23
  79.1 2.8 %collective-permute-start.8 = (bf16[2,640,128]{2,1,0:T(8,128)(2,1)}, bf16[2,640,128]{2,1,0:T(8,128)(2,1)}, u32[]{:S(2)}, u32[]{:S(2)}) collective-permute-start(bf16[2,640,128]{2,1,0:T(8,128)(2,1)} %slice.23), channel_id=1, source_target_pairs={{0,96},{32,0},{64,32},{96,64},{1,97},{33,1},{65,33},{97,65},{2,98}... | collective-permute-start | bytes 983048 | tf_op jit(solution)/shard_map/ppermute | solution.py:34
  81.9 0.0 collective-permute-done.7.old_3
  81.9 0.8 slice.24
  82.7 0.0 collective-permute-start.9
  82.7 0.1 slice.22
  82.7 0.0 collective-permute-start.1
  82.8 4.8 %all-to-all-done.2 = f32[128,1,128]{2,1,0:T(1,128)S(1)} async-done(((f32[128,1,128]{2,1,0:T(1,128)}), f32[128,1,128]{2,1,0:T(1,128)S(1)}, u32[]{:S(2)}, u32[]{:S(2)}) %all-to-all-start.2) | async-done | bytes 65568 | tf_op jit(solution)/shard_map/all_to_all | solution.py:39
  87.6 0.7 slice_reduce_fusion
  89.0 0.0 collective-permute-done.1
  89.0 1.4 %divide_convert_fusion.1 = (bf16[16,320]{1,0:T(8,128)(2,1)S(1)}, f32[16,320]{1,0:T(8,128)}, f32[16,320]{1,0:T(8,128)}, bf16[16,320]{1,0:T(8,128)(2,1)S(1)}, f32[16,320]{1,0:T(8,128)}, /*index=5*/f32[16,320]{1,0:T(8,128)}) fusion(f32[16,320]{1,0:T(8,128)S(1)} %collective-permute-done.1, f32[16,640]{1,0:T(8,128)S(1)} %convert_reduce_fusion, pred[]{:T(512)S(6)} %eq.3, ...), kind=kLoop, calls=%fused_computation.12 | loop fusion | flops 122880 | bytes 225285 | tf_op jit(solution)/shard_map/convert_element_type | solution.py:132
  90.4 0.1 pad_maximum_fusion.1
  90.5 0.8 broadcast_in_dim.7
  91.3 3.5 %all-to-all-start.3 = ((bf16[16,16,640]{2,1,0:T(8,128)(2,1)}), bf16[16,16,640]{2,1,0:T(8,128)(2,1)S(1)}, u32[]{:S(2)}, u32[]{:S(2)}) async-start(bf16[16,16,640]{2,1,0:T(8,128)(2,1)} %broadcast_in_dim.7), calls=%async_computation.3 | async-start | bytes 655360 | tf_op jit(solution)/shard_map/all_to_all | solution.py:39
  94.8 0.0 collective-permute-done.8.old_2a
  94.8 0.0 collective-permute-done.9.old_2b
  94.8 9.5 %all-to-all-done.3 = bf16[16,16,640]{2,1,0:T(8,128)(2,1)S(1)} async-done(((bf16[16,16,640]{2,1,0:T(8,128)(2,1)}), bf16[16,16,640]{2,1,0:T(8,128)(2,1)S(1)}, u32[]{:S(2)}, u32[]{:S(2)}) %all-to-all-start.3) | async-done | bytes 327712 | tf_op jit(solution)/shard_map/all_to_all | solution.py:39
  104.3 0.0 collective-permute-done.2.basis_other
  104.3 0.0 copy-done.8
  104.4 0.0 copy-start.3
  104.4 0.9 copy-done.3
  105.3 0.0 copy-start.5
  105.3 0.8 copy-done.5
  106.1 0.0 copy-start.7
  106.1 0.8 copy-done.7
  106.9 6.2 %final.1 = (f32[320,128]{1,0:T(8,128)}, f32[320,128]{1,0:T(8,128)}, bf16[320,2048]{1,0:T(8,128)(2,1)}, f32[320,128]{1,0:T(8,128)}, f32[320,128]{1,0:T(8,128)}, /*index=5*/bf16[320,2048]{1,0:T(8,128)(2,1)}) custom-call(s32[6]{0:T(128)S(1)} %copy-done.8, bf16[256,640]{1,0:T(8,128)(2,1)S(1)} %bitcast.22, bf16[128,256]{1,0:T(8,128)(2,1)S(1)} %copy-done.5, ...), custom_call_target="tpu_custom_call" | custom-call | flops 700000000 | bytes 10000000 | tf_op jit(solution)/shard_map/final/pallas_call | solution.py:211
  (2 shorter events, 0.0 us)
Async XLA Ops:
  1.3 13.0 %copy-start.4 = (bf16[128,256]{1,0:T(8,128)(2,1)S(1)}, bf16[128,256]{1,0:T(8,128)(2,1)}, u32[]{:S(2)}) copy-start(bf16[128,256]{1,0:T(8,128)(2,1)} %b_in.1) | copy-start | bytes 196612
  1.3 13.0 %copy-start.6 = (bf16[128,256]{1,0:T(8,128)(2,1)S(1)}, bf16[128,256]{1,0:T(8,128)(2,1)}, u32[]{:S(2)}) copy-start(bf16[128,256]{1,0:T(8,128)(2,1)} %b_out.1) | copy-start | bytes 196612
  14.2 35.3 %collective-permute-start = (bf16[320,2048]{1,0:T(8,128)(2,1)}, bf16[320,2048]{1,0:T(8,128)(2,1)}, u32[]{:S(2)}, u32[]{:S(2)}) collective-permute-start(bf16[320,2048]{1,0:T(8,128)(2,1)} %get-tuple-element.19), channel_id=1, source_target_pairs={{0,1},{1,0},{2,3},{3,2},{4,5},{5,4},{6,7},{7,6},{8,9},{9,8},{10,11... | collective-permute-start | bytes 3932168 | tf_op jit(solution)/shard_map/ppermute | solution.py:30
  15.4 8.1 %copy-start.1 = (f32[128,320]{0,1:T(8,128)S(1)}, f32[128,320]{0,1:T(8,128)}, u32[]{:S(2)}) copy-start(f32[128,320]{0,1:T(8,128)} %param.18) | copy-start | bytes 491524
  15.4 8.1 %copy-start.2 = (f32[320,128]{1,0:T(8,128)S(1)}, f32[320,128]{1,0:T(8,128)}, u32[]{:S(2)}) copy-start(f32[320,128]{1,0:T(8,128)} %w_out.3) | copy-start | bytes 491524
  15.4 34.1 %all-to-all-start = ((bf16[16,128,256]{2,1,0:T(8,128)(2,1)}), bf16[16,128,256]{2,1,0:T(8,128)(2,1)S(1)}, u32[]{:S(2)}, u32[]{:S(2)}) async-start(bf16[16,128,256]{2,1,0:T(8,128)(2,1)} %broadcast_in_dim.6), calls=%async_computation | async-start | bytes 2097152 | tf_op jit(solution)/shard_map/all_to_all | solution.py:39
  23.5 18.5 %collective-permute-start.3 = (bf16[640,128]{1,0:T(8,128)(2,1)S(1)}, bf16[640,128]{1,0:T(8,128)(2,1)S(1)}, u32[]{:S(2)}, u32[]{:S(2)}) collective-permute-start(bf16[640,128]{1,0:T(8,128)(2,1)S(1)} %pack.1), channel_id=1, source_target_pairs={{0,24},{8,0},{16,8},{24,16},{1,25},{9,1},{17,9},{25,17},{2,26},{10... | collective-permute-start | bytes 491528 | tf_op jit(solution)/shard_map/ppermute | solution.py:34
  26.7 15.6 %collective-permute-start.4 = (bf16[640,128]{1,0:T(8,128)(2,1)S(1)}, bf16[640,128]{1,0:T(8,128)(2,1)S(1)}, u32[]{:S(2)}, u32[]{:S(2)}) collective-permute-start(bf16[640,128]{1,0:T(8,128)(2,1)S(1)} %pack.1), channel_id=1, source_target_pairs={{0,8},{8,16},{16,24},{24,0},{1,9},{9,17},{17,25},{25,1},{2,10},{10... | collective-permute-start | bytes 491528 | tf_op jit(solution)/shard_map/ppermute | solution.py:34
  26.7 20.3 %collective-permute-start.5 = (bf16[640,128]{1,0:T(8,128)(2,1)S(1)}, bf16[640,128]{1,0:T(8,128)(2,1)S(1)}, u32[]{:S(2)}, u32[]{:S(2)}) collective-permute-start(bf16[640,128]{1,0:T(8,128)(2,1)S(1)} %pack.1), channel_id=1, source_target_pairs={{0,16},{8,24},{16,0},{24,8},{1,17},{9,25},{17,1},{25,9},{2,18},{10... | collective-permute-start | bytes 491528 | tf_op jit(solution)/shard_map/ppermute | solution.py:34
  47.1 31.2 %collective-permute-start.6 = (bf16[4,640,128]{2,1,0:T(8,128)(2,1)S(1)}, bf16[4,640,128]{2,1,0:T(8,128)(2,1)S(1)}, u32[]{:S(2)}, u32[]{:S(2)}) collective-permute-start(bf16[4,640,128]{2,1,0:T(8,128)(2,1)S(1)} %pad_maximum_fusion.old_0), channel_id=1, source_target_pairs={{0,96},{32,0},{64,32},{96,64},{1,97},{33,1},{65,33},{97,65},{2,98}... | collective-permute-start | bytes 1966088 | tf_op jit(solution)/shard_map/ppermute | solution.py:34
  49.5 32.4 %collective-permute-start.7 = (bf16[4,640,128]{2,1,0:T(8,128)(2,1)S(1)}, bf16[4,640,128]{2,1,0:T(8,128)(2,1)S(1)}, u32[]{:S(2)}, u32[]{:S(2)}) collective-permute-start(bf16[4,640,128]{2,1,0:T(8,128)(2,1)S(1)} %pad_maximum_fusion.old_0), channel_id=1, source_target_pairs={{0,32},{32,64},{64,96},{96,0},{1,33},{33,65},{65,97},{97,1},{2,34}... | collective-permute-start | bytes 1966088 | tf_op jit(solution)/shard_map/ppermute | solution.py:34
  49.5 1.3 %copy-start = (bf16[320,2048]{1,0:T(8,128)(2,1)S(1)}, bf16[320,2048]{1,0:T(8,128)(2,1)}, u32[]{:S(2)}) copy-start(bf16[320,2048]{1,0:T(8,128)(2,1)} %get-tuple-element.18.kept) | copy-start | bytes 3932164
  55.0 15.0 %all-to-all-start.1 = ((bf16[16,16,640]{2,1,0:T(8,128)(2,1)}), bf16[16,16,640]{2,1,0:T(8,128)(2,1)S(1)}, u32[]{:S(2)}, u32[]{:S(2)}) async-start(bf16[16,16,640]{2,1,0:T(8,128)(2,1)} %bitcast.9), calls=%async_computation.1 | async-start | bytes 655360 | tf_op jit(solution)/shard_map/all_to_all | solution.py:288
  60.1 44.2 %collective-permute-start.2 = (bf16[2048,256]{1,0:T(8,128)(2,1)S(1)}, bf16[2048,256]{1,0:T(8,128)(2,1)}, u32[]{:S(2)}, u32[]{:S(2)}) collective-permute-start(bf16[2048,256]{1,0:T(8,128)(2,1)S(1)} %bitcast.20), channel_id=1, source_target_pairs={{0,1},{1,0},{2,3},{3,2},{4,5},{5,4},{6,7},{7,6},{8,9},{9,8},{10,11... | collective-permute-start | bytes 3145736 | tf_op jit(solution)/shard_map/ppermute | solution.py:30
  71.9 15.7 %all-to-all-start.2 = ((f32[128,1,128]{2,1,0:T(1,128)}), f32[128,1,128]{2,1,0:T(1,128)S(1)}, u32[]{:S(2)}, u32[]{:S(2)}) async-start(f32[128,1,128]{2,1,0:T(1,128)} %broadcast_in_dim_broadcast_in_dim.3), calls=%async_computation.2 | async-start | bytes 131072 | tf_op jit(solution)/shard_map/all_to_all | solution.py:39
  78.3 26.1 %copy-start.8 = (s32[6]{0:T(128)S(1)}, s32[6]{0:T(128)}, u32[]{:S(2)}) copy-start(s32[6]{0:T(128)} %stack.42.where) | copy-start | bytes 76
  79.1 15.8 %collective-permute-start.8 = (bf16[2,640,128]{2,1,0:T(8,128)(2,1)}, bf16[2,640,128]{2,1,0:T(8,128)(2,1)}, u32[]{:S(2)}, u32[]{:S(2)}) collective-permute-start(bf16[2,640,128]{2,1,0:T(8,128)(2,1)} %slice.23), channel_id=1, source_target_pairs={{0,96},{32,0},{64,32},{96,64},{1,97},{33,1},{65,33},{97,65},{2,98}... | collective-permute-start | bytes 983048 | tf_op jit(solution)/shard_map/ppermute | solution.py:34
  82.7 12.2 %collective-permute-start.9 = (bf16[2,640,128]{2,1,0:T(8,128)(2,1)}, bf16[2,640,128]{2,1,0:T(8,128)(2,1)}, u32[]{:S(2)}, u32[]{:S(2)}) collective-permute-start(bf16[2,640,128]{2,1,0:T(8,128)(2,1)} %slice.24), channel_id=1, source_target_pairs={{0,32},{32,64},{64,96},{96,0},{1,33},{33,65},{65,97},{97,1},{2,34}... | collective-permute-start | bytes 983048 | tf_op jit(solution)/shard_map/ppermute | solution.py:34
  82.7 6.2 %collective-permute-start.1 = (f32[16,320]{1,0:T(8,128)S(1)}, f32[16,320]{1,0:T(8,128)S(1)}, u32[]{:S(2)}, u32[]{:S(2)}) collective-permute-start(f32[16,320]{1,0:T(8,128)S(1)} %slice.22), channel_id=1, source_target_pairs={{0,1},{1,0},{2,3},{3,2},{4,5},{5,4},{6,7},{7,6},{8,9},{9,8},{10,11... | collective-permute-start | bytes 61448 | tf_op jit(solution)/shard_map/ppermute | solution.py:30
  91.3 13.1 %all-to-all-start.3 = ((bf16[16,16,640]{2,1,0:T(8,128)(2,1)}), bf16[16,16,640]{2,1,0:T(8,128)(2,1)S(1)}, u32[]{:S(2)}, u32[]{:S(2)}) async-start(bf16[16,16,640]{2,1,0:T(8,128)(2,1)} %broadcast_in_dim.7), calls=%async_computation.3 | async-start | bytes 655360 | tf_op jit(solution)/shard_map/all_to_all | solution.py:39
  104.4 0.9 copy-start.3
  105.3 0.8 copy-start.5
  106.1 0.8 copy-start.7
where the time goes:
time: 114 us; the launch traced here: 113 us
  waiting for transfers between devices  42 us (37%)
  starting transfers between devices  34 us (30%)
  Pallas kernels  23.3 us (20%)
  local copies, waits for them, and re-layouts  9.26 us (8%)
  other arithmetic  3.01 us (3%)
  between operations  1.53 us (1%)
    all_to_all x3, starting transfers between devices, sent_to_all(): return lax.all_to_all(copies, axis, split_axis=0, concat_axis=0, tiled=True)  18 us
    ppermute x7, waiting for transfers between devices, shifted(): lax.ppermute(array, axis, [(i, (i + by) % SIDE) for i in range(SIDE)])  18 us
    all_to_all x3, waiting for transfers between devices, sent_to_all(): return lax.all_to_all(copies, axis, split_axis=0, concat_axis=0, tiled=True)  14.3 us
    pallas_call x1, Pallas kernels, grads(): pl.pallas_call(grads_kernel, grid=(2048 // tile,), in_specs=[SMEM, wide,...  13 us
    ppermute x7, starting transfers between devices, shifted(): lax.ppermute(array, axis, [(i, (i + by) % SIDE) for i in range(SIDE)])  10.7 us
    all_to_all x1, waiting for transfers between devices, shards(): lax.all_to_all(part.reshape(PEERS, ROWS, 2 * W), FS, split_axis=0, concat...  9.7 us
    pallas_call x1, Pallas kernels, final(): pl.pallas_call(final_kernel, grid_spec=pltpu.PrefetchScalarGridSpec(num_s...  6.16 us
    all_to_all x1, starting transfers between devices, shards(): lax.all_to_all(part.reshape(PEERS, ROWS, 2 * W), FS, split_axis=0, concat...  5.15 us
  transfers between devices with their start and end apart: 14, of which 6 were waited for; matrix products, arithmetic and copies ran while one was open for 7% of the time, Pallas kernels for 4%

commit v1 on v0

v1 whole, which is shorter than its diff:
```python
import functools
import math

import jax
import jax.numpy as jnp
from jax import lax
from jax.experimental import pallas as pl
from jax.experimental.pallas import tpu as pltpu
from jax.sharding import Mesh
from jax.sharding import PartitionSpec as P

D_RNN = 2560
RANK = 256
FS = ("fs_0", "fs_1")
TP = ("tp_0", "tp_1")
EVERY = ("fs_0", "fs_1", "tp_0", "tp_1")
BF16 = jnp.bfloat16
F32 = jnp.float32

W = 320
ROWS = 16
PEERS = 16
SIDE = 4

LIMIT = pltpu.CompilerParams(vmem_limit_bytes=20 << 20)
VMEM = pl.BlockSpec(memory_space=pltpu.VMEM)
SMEM = pl.BlockSpec(memory_space=pltpu.SMEM)


def swapped(array):
    return lax.ppermute(array, "tp_1", [(0, 1), (1, 0)])


def shifted(array, axis, by):
    return lax.ppermute(array, axis, [(i, (i + by) % SIDE) for i in range(SIDE)])


def contract(a, b, dims):
    return lax.dot_general(a, b, (dims, ((), ())), preferred_element_type=F32)


def pack_kernel(core, w_in, w_out, b_in, b_out, weights, bases):
    weights[0:W, :] = w_in[...].astype(BF16)
    weights[W : 2 * W, :] = w_out[...].astype(BF16)
    mine = jnp.where(core[0] == 0, b_in[...], b_out[...])
    for i in range(PEERS):
        bases[i] = mine


def pack(*args):
    return pl.pallas_call(
        pack_kernel,
        out_shape=(
            jax.ShapeDtypeStruct((2 * W, 128), BF16),
            jax.ShapeDtypeStruct((PEERS, 128, RANK), BF16),
        ),
        grid=(1,),
        in_specs=[
            SMEM,
            pl.BlockSpec((W, 128), lambda i: (0, 0)),
            pl.BlockSpec((W, 128), lambda i: (0, 0)),
            pl.BlockSpec((128, RANK), lambda i: (0, 0)),
            pl.BlockSpec((128, RANK), lambda i: (0, 0)),
        ],
        out_specs=(
            pl.BlockSpec((2 * W, 128), lambda i: (0, 0)),
            pl.BlockSpec((PEERS, 128, RANK), lambda i: (0, 0, 0)),
        ),
        name="pack",
        cost_estimate=pl.CostEstimate(flops=10**6, bytes_accessed=500_000, transcendentals=0),
    )(*args)


GRAD_TILE = 512
GRAD_TILES = 2048 // GRAD_TILE


def grad_kernel(flip, core, conv, lru, h, o, out, wide, tall, sems):
    uses_in = core[0] == flip

    def tile(source, k):
        cols = slice(k * GRAD_TILE, (k + 1) * GRAD_TILE)
        return pltpu.make_async_copy(source.at[:, cols], tall.at[k], sems.at[k])

    def factor(source):
        return pltpu.make_async_copy(source, wide, sems.at[GRAD_TILES])

    @pl.when(uses_in)
    def _():
        factor(conv).start()
        for k in range(GRAD_TILES):
            tile(h, k).start()

    @pl.when(jnp.logical_not(uses_in))
    def _():
        factor(lru).start()
        for k in range(GRAD_TILES):
            tile(o, k).start()

    factor(conv).wait()
    for k in range(GRAD_TILES):
        tile(h, k).wait()
        out[:, k * GRAD_TILE : (k + 1) * GRAD_TILE] = jnp.dot(
            wide[...], tall[k], preferred_element_type=F32
        ).astype(BF16)


def grad(flip, core, conv, lru, h, o):
    return pl.pallas_call(
        functools.partial(grad_kernel, flip),
        in_specs=[SMEM] + [pl.BlockSpec(memory_space=pltpu.HBM)] * 4,
        out_specs=VMEM,
        out_shape=jax.ShapeDtypeStruct((W, 2048), BF16),
        scratch_shapes=[
            pltpu.VMEM((W, 2048), BF16),
            pltpu.VMEM((GRAD_TILES, 2048, GRAD_TILE), BF16),
            pltpu.SemaphoreType.DMA((GRAD_TILES + 1,)),
        ],
        name="grad",
        compiler_params=pltpu.CompilerParams(vmem_limit_bytes=63 << 20),
        cost_estimate=pl.CostEstimate(
            flops=2 * 2048 * 2048 * W, bytes_accessed=11_000_000, transcendentals=0
        ),
    )(core, conv, lru, h, o)


PROJECT_TILES = 4


def project_kernel(kept, came, basis, out, kept_in, came_in, basis_in, sems):
    depth = 2048 // PROJECT_TILES
    copies = []
    for k in range(PROJECT_TILES):
        at = slice(k * depth, (k + 1) * depth)
        copies.append(
            (
                pltpu.make_async_copy(basis.at[at], basis_in.at[k], sems.at[0, k]),
                pltpu.make_async_copy(kept.at[:, at], kept_in.at[k], sems.at[1, k]),
                pltpu.make_async_copy(came.at[:, at], came_in.at[k], sems.at[2, k]),
            )
        )
    for group in copies:
        for copy in group:
            copy.start()
    mine = jnp.zeros((W, RANK), F32)
    other = jnp.zeros((W, RANK), F32)
    for k in range(PROJECT_TILES):
        for copy in copies[k]:
            copy.wait()
        mine = mine + jnp.dot(kept_in[k], basis_in[k], preferred_element_type=F32)
        other = other + jnp.dot(came_in[k], basis_in[k], preferred_element_type=F32)
    out[:, 0:W] = mine.T.astype(BF16)
    out[:, W:] = other.T.astype(BF16)


def project(kept, came, basis):
    depth = 2048 // PROJECT_TILES
    return pl.pallas_call(
        project_kernel,
        in_specs=[pl.BlockSpec(memory_space=pltpu.HBM)] * 3,
        out_specs=VMEM,
        out_shape=jax.ShapeDtypeStruct((RANK, 2 * W), BF16),
        scratch_shapes=[
            pltpu.VMEM((PROJECT_TILES, W, depth), BF16),
            pltpu.VMEM((PROJECT_TILES, W, depth), BF16),
            pltpu.VMEM((PROJECT_TILES, depth, RANK), BF16),
            pltpu.SemaphoreType.DMA((3, PROJECT_TILES)),
        ],
        name="project",
        compiler_params=pltpu.CompilerParams(vmem_limit_bytes=63 << 20),
        cost_estimate=pl.CostEstimate(
            flops=4 * 2048 * RANK * W, bytes_accessed=4_000_000, transcendentals=0
        ),
    )(kept, came, basis)


def collect_kernel(arrived, kept, given, squares):
    total = arrived[0].astype(F32)
    for i in range(1, PEERS):
        total = total + arrived[i].astype(F32)
    kept[...] = total[:, 0:W]
    given[...] = total[:, W:]
    sum_ = jnp.sum(jnp.sum(total * total, axis=0, keepdims=True), axis=1, keepdims=True)
    squares[...] = jnp.broadcast_to(sum_.reshape(1, 1, 1), (128, 1, 128))


def collect(arrived):
    return pl.pallas_call(
        collect_kernel,
        out_shape=(
            jax.ShapeDtypeStruct((ROWS, W), F32),
            jax.ShapeDtypeStruct((ROWS, W), F32),
            jax.ShapeDtypeStruct((128, 1, 128), F32),
        ),
        in_specs=[VMEM],
        out_specs=(VMEM,) * 3,
        name="collect",
        compiler_params=LIMIT,
        cost_estimate=pl.CostEstimate(flops=10**6, bytes_accessed=500_000, transcendentals=0),
    )(arrived)


def apply_kernel(
    core, totals, kept, came, old, nf_in, nv_in, nf_out, nv_out, dirs
):
    takes_in = core[0] == 0
    total = jnp.sum(totals[...], axis=0)[:, 0:1]
    factor = math.sqrt(2.0 * RANK * D_RNN) * lax.rsqrt(total + 1e-06)
    mine = kept[...]
    other = came[...]

    def moments(scaled, at, new_first, new_second):
        first = 0.8 * old[at : at + ROWS] + 0.2 * scaled
        second = 0.9 * old[at + ROWS : at + 2 * ROWS] + 0.1 * scaled * scaled
        new_first[...] = first
        new_second[...] = second
        return (first / (jnp.sqrt(second) + 1e-08)).astype(BF16)

    both = jnp.concatenate(
        (
            moments(factor * jnp.where(takes_in, mine, other), 0, nf_in, nv_in),
            moments(factor * jnp.where(takes_in, other, mine), 2 * ROWS, nf_out, nv_out),
        ),
        axis=1,
    )
    for i in range(PEERS):
        dirs[i] = both


def apply(*args):
    row = jax.ShapeDtypeStruct((ROWS, W), F32)
    return pl.pallas_call(
        apply_kernel,
        out_shape=(row, row, row, row, jax.ShapeDtypeStruct((PEERS, ROWS, 2 * W), BF16)),
        in_specs=[SMEM] + [VMEM] * 4,
        out_specs=(VMEM,) * 5,
        name="apply",
        compiler_params=LIMIT,
        cost_estimate=pl.CostEstimate(flops=10**6, bytes_accessed=500_000, transcendentals=0),
    )(*args)


def swap_last(n):
    return n ^ (n >> 1)


def final_kernel(
    core,
    at_x,
    at_z,
    full,
    bases,
    weights,
    basis_own,
    basis_other,
    old_0a,
    old_0b,
    old_1a,
    old_1b,
    old_3a,
    old_3b,
    old_2a,
    old_2b,
    step_in,
    new_in,
    copy_in,
    step_out,
    new_out,
    copy_out,
    turned,
):
    takes_in = core[0] == 0
    n = pl.program_id(0)

    @pl.when(n == 0)
    def _():
        turned[...] = full[...].astype(F32).T.astype(BF16)
        own_in = contract(turned[0:W], bases[0:128], ((1,), (1,)))
        own_out = contract(turned[W:], bases[128:], ((1,), (1,)))
        step_in[...] = own_in
        step_out[...] = own_out
        new_in[...] = weights[0:W] - 0.02 * own_in
        new_out[...] = weights[W:] - 0.02 * own_out

    own = basis_own[...]
    other = basis_other[...]

    def write(block_of):
        s_in = contract(turned[0:W], jnp.where(takes_in, own, other), ((1,), (1,)))
        s_out = contract(turned[W:], jnp.where(takes_in, other, own), ((1,), (1,)))
        for k in range(SIDE):
            block = block_of(swap_last((k - at_x[0]) & (SIDE - 1))).astype(F32)
            cols = slice(128 * k, 128 * (k + 1))
            copy_in[:, cols] = (block[0:W] - 0.02 * s_in[:, cols]).astype(BF16)
            copy_out[:, cols] = (block[W:] - 0.02 * s_out[:, cols]).astype(BF16)

    pairs = ((old_0a, old_0b), (old_1a, old_1b), (old_3a, old_3b), (old_2a, old_2b))
    for step, (near, far) in enumerate(pairs):

        @pl.when(n == step)
        def _():
            write(lambda r: jnp.where(r < 2, near[r & 1], far[r & 1]))


def final(core, at_x, at_z, full, bases, weights, own, other, old):
    shape = jax.ShapeDtypeStruct

    def whole(s):
        return pl.BlockSpec(s, lambda *_: (0,) * len(s))

    def place(i, at_z):
        return (at_z[0] + swap_last(i)) & (SIDE - 1)

    tall = whole((W, 128))
    tile = pl.BlockSpec((512, RANK), lambda i, core, at_x, at_z: (place(i, at_z), 0))
    copy = pl.BlockSpec((W, 512), lambda i, core, at_x, at_z: (0, place(i, at_z)))
    return pl.pallas_call(
        final_kernel,
        grid_spec=pltpu.PrefetchScalarGridSpec(
            num_scalar_prefetch=3,
            grid=(SIDE,),
            in_specs=[
                whole((RANK, 2 * W)),
                whole((2 * 128, RANK)),
                whole((2 * W, 128)),
                tile,
                tile,
                *[whole((2, 2 * W, 128))] * 8,
            ],
            out_specs=(tall, tall, copy, tall, tall, copy),
            scratch_shapes=[pltpu.VMEM((2 * W, RANK), BF16)],
        ),
        out_shape=(
            shape((W, 128), F32),
            shape((W, 128), F32),
            shape((W, 2048), BF16),
            shape((W, 128), F32),
            shape((W, 128), F32),
            shape((W, 2048), BF16),
        ),
        name="final",
        compiler_params=LIMIT,
        cost_estimate=pl.CostEstimate(
            flops=700_000_000, bytes_accessed=10_000_000, transcendentals=0
        ),
    )(core, at_x, at_z, full, bases, weights, own, other, *old)


def shards(
    h_saved,
    conv_cotan,
    lru_out,
    out_cotan,
    basis_in,
    basis_out,
    weight_in,
    weight_out,
    first_in,
    second_in,
    first_out,
    second_out,
):
    core = lax.axis_index("tp_1").astype(jnp.int32).reshape(1)
    at_z = lax.axis_index("fs_0").astype(jnp.int32).reshape(1)
    at_x = lax.axis_index("fs_1").astype(jnp.int32).reshape(1)

    packed, bases = pack(core, weight_in.T, weight_out, basis_in, basis_out)

    basis_own = lax.all_to_all(bases, FS, 0, 0, tiled=True).reshape(-1, RANK)
    basis_other = swapped(basis_own)

    pieces = [packed]
    for d in (1, 3, 2):
        pieces.append(shifted(packed, "fs_1", -d))
    halves = [lax.optimization_barrier(jnp.stack(pieces[k : k + 2])) for k in (0, 2)]
    old = list(halves)
    for d in (1, 3):
        for k in range(2):
            old.append(shifted(halves[k], "fs_0", -d))
    old.append(shifted(old[2], "fs_0", -1))
    old.append(shifted(old[5], "fs_0", -3))

    wide = (conv_cotan.T, lru_out.T, h_saved, out_cotan)
    given = grad(1, core, *wide)
    came = swapped(given)
    kept = grad(0, core, *wide)
    part = project(kept, came, basis_own)
    arrived = lax.all_to_all(
        part.reshape(PEERS, ROWS, 2 * W), FS, split_axis=0, concat_axis=0, tiled=True
    )
    old_moments = lax.optimization_barrier(
        jnp.concatenate((first_in, second_in, first_out, second_out), axis=0)
    )
    old_weights = lax.optimization_barrier(
        jnp.concatenate((weight_in.T, weight_out), axis=0)
    )
    own_bases = lax.optimization_barrier(jnp.concatenate((basis_in, basis_out), axis=0))
    proj_own, proj_given, squares = collect(arrived)
    totals = lax.all_to_all(squares, EVERY, 0, 0, tiled=True)
    proj_other = swapped(proj_given)
    first_a, second_a, first_b, second_b, dirs = apply(
        core, totals, proj_own, proj_other, old_moments
    )
    full = lax.all_to_all(dirs, FS, 0, 0, tiled=True).reshape(RANK, 2 * W)
    step_in, new_in, copy_in, step_out, new_out, copy_out = final(
        core, at_x, at_z, full, own_bases, old_weights, basis_own, basis_other, old
    )
    return (
        step_in.T,
        new_in.T,
        copy_in.T,
        first_a,
        second_a,
        step_out,
        new_out,
        copy_out,
        first_b,
        second_b,
    )


def solution(mesh):
    finer = Mesh(mesh.devices.reshape(4, 4, 4, 2), EVERY)
    placed = (
        P(FS, None),
        P(FS, TP),
        P(FS, TP),
        P(FS, None),
        P(FS, None),
        P(FS, None),
        P(FS, TP),
        P(TP, FS),
        P(FS, TP),
        P(FS, TP),
        P(FS, TP),
        P(FS, TP),
    )
    return jax.shard_map(
        shards,
        mesh=finer,
        in_specs=placed,
        out_specs=(
            P(FS, TP),
            P(FS, TP),
            P(None, TP),
            P(FS, TP),
            P(FS, TP),
            P(TP, FS),
            P(TP, FS),
            P(TP, None),
            P(FS, TP),
            P(FS, TP),
        ),
        check_vma=False,
    )
```

time: 114 us -> 99 us (0.87)
  waiting for transfers between devices: 42 us -> 28.8 us
  local copies, waits for them, and re-layouts: 9.26 us -> 0.67 us
  starting transfers between devices: 34 us -> 38.7 us
  Pallas kernels: 23.3 us -> 25.6 us
    ppermute x7 -> x9, waiting for transfers between devices: 18 us -> 7.48 us  [shifted(): lax.ppermute(array, axis, [(i, (i + by) % SIDE) for i in range(SIDE)])]
    ppermute x7 -> x9, starting transfers between devices: 10.7 us -> 15.6 us  [shifted(): lax.ppermute(array, axis, [(i, (i + by) % SIDE) for i in range(SIDE)])]
    all_to_all x1, waiting for transfers between devices: 9.7 us -> 6.17 us  [shards(): lax.all_to_all(part.reshape(PEERS, ROWS, 2 * W), FS, split_axis=0, concat...]
    unnamed x18 -> x4, local copies, waits for them, and re-layouts: 3.93 us -> 0.67 us
    pallas_call x3 -> x6, Pallas kernels: 17.1 us -> 20.3 us  [the longest x2 12.9 us: grad(): pl.pallas_call(functools.partial(grad_kernel, flip), in_specs=[SMEM] + [p...]
    concatenate x1 -> x3, other arithmetic: 0.08 us -> 2.7 us  [the longest x1 1.02 us: shards(): jnp.concatenate((weight_in.T, weight_out), axis=0)]
    another operation x2 -> x0, local copies, waits for them, and re-layouts: 1.91 us -> none  [the longest x1 1.31 us: sent_to_all(): copies = jnp.broadcast_to(array, (lax.axis_size(axis), *array.shape))]
    broadcast_in_dim x2 -> x0, local copies, waits for them, and re-layouts: 1.82 us -> none  [sent_to_all(): copies = jnp.broadcast_to(array, (lax.axis_size(axis), *array.shape))]
  transfers between devices with their start and end apart: 14 -> 16, of which waited for: 6 -> 6; matrix products, arithmetic and copies ran while one was open for 7% -> 4% of each run, Pallas kernels for 4% -> 14%
where the time goes in v1:
time: 99 us; the launch traced here: 98.3 us
  starting transfers between devices  38.7 us (39%)
  waiting for transfers between devices  28.8 us (29%)
  Pallas kernels  25.6 us (26%)
  other arithmetic  3.76 us (4%)
    ppermute x9, starting transfers between devices, shifted(): lax.ppermute(array, axis, [(i, (i + by) % SIDE) for i in range(SIDE)])  15.6 us
    pallas_call x2, Pallas kernels, grad(): pl.pallas_call(functools.partial(grad_kernel, flip), in_specs=[SMEM] + [p...  12.9 us
    all_to_all x1, starting transfers between devices, shards(): basis_own = lax.all_to_all(bases, FS, 0, 0, tiled=True).reshape(-1, RANK)  8.17 us
    ppermute x9, waiting for transfers between devices, shifted(): lax.ppermute(array, axis, [(i, (i + by) % SIDE) for i in range(SIDE)])  7.48 us
    all_to_all x1, starting transfers between devices, shards(): totals = lax.all_to_all(squares, EVERY, 0, 0, tiled=True)  6.68 us
    all_to_all x1, waiting for transfers between devices, shards(): basis_own = lax.all_to_all(bases, FS, 0, 0, tiled=True).reshape(-1, RANK)  6.58 us
    all_to_all x1, waiting for transfers between devices, shards(): lax.all_to_all(part.reshape(PEERS, ROWS, 2 * W), FS, split_axis=0, concat...  6.17 us
    pallas_call x1, Pallas kernels, final(): pl.pallas_call(final_kernel, grid_spec=pltpu.PrefetchScalarGridSpec(num_s...  5.3 us
  transfers between devices with their start and end apart: 16, of which 6 were waited for; matrix products, arithmetic and copies ran while one was open for 4% of the time, Pallas kernels for 14%

profile of v1, /device:TPU:0, one launch (start us, length us, event | category | flops | bytes accessed | tf_op | source)
XLA Modules:
  0.0 98.3 jit_solution(10824426216326647982)
XLA Ops:
  0.6 6.5 %grad.3 = bf16[320,2048]{1,0:T(8,128)(2,1)} custom-call(s32[1]{0:T(128)} %bitcast.core, bf16[320,2048]{1,0:T(8,128)(2,1)} %bitcast.17, bf16[320,2048]{1,0:T(8,128)(2,1)} %bitcast.19, bf16[2048,2048]{1,0:T(8,128)(2,1)} %h.3, bf16[2048,2048]{1,0:T(8,128)(2,1)} %o.3), custom_call_target="tpu_custom_call" | custom-call | flops 2684354560 | bytes 11000000 | tf_op jit(solution)/shard_map/grad/pallas_call | solution.py:109
  7.1 0.1 collective-permute-start
  7.2 2.1 %pack.1 = (bf16[640,128]{1,0:T(8,128)(2,1)}, bf16[16,128,256]{2,1,0:T(8,128)(2,1)}) custom-call(s32[1]{0:T(128)} %bitcast.core, f32[320,128]{1,0:T(8,128)} %bitcast.22, f32[320,128]{1,0:T(8,128)} %w_out.1, bf16[128,256]{1,0:T(8,128)(2,1)} %b_in.1, bf16[128,256]{1,0:T(8,128)(2,1)} %b_out.1), custom_call_target="tpu_custom_call" | custom-call | flops 1000000 | bytes 500000 | tf_op jit(solution)/shard_map/pack/pallas_call | solution.py:51
  9.4 0.0 copy-start
  9.4 8.2 %all-to-all-start = ((bf16[16,128,256]{2,1,0:T(8,128)(2,1)}), bf16[16,128,256]{2,1,0:T(8,128)(2,1)}, u32[]{:S(2)}, u32[]{:S(2)}) async-start(bf16[16,128,256]{2,1,0:T(8,128)(2,1)} %get-tuple-element.26), calls=%async_computation | async-start | bytes 2097152 | tf_op jit(solution)/shard_map/all_to_all | solution.py:369
  17.5 0.0 copy-done
  17.5 1.9 %collective-permute-start.4 = (bf16[640,128]{1,0:T(8,128)(2,1)S(1)}, bf16[640,128]{1,0:T(8,128)(2,1)S(1)}, u32[]{:S(2)}, u32[]{:S(2)}) collective-permute-start(bf16[640,128]{1,0:T(8,128)(2,1)S(1)} %copy-done), channel_id=1, source_target_pairs={{0,8},{8,16},{16,24},{24,0},{1,9},{9,17},{17,25},{25,1},{2,10},{10... | collective-permute-start | bytes 491528 | tf_op jit(solution)/shard_map/ppermute | solution.py:35
  19.5 2.7 %collective-permute-start.5 = (bf16[640,128]{1,0:T(8,128)(2,1)S(1)}, bf16[640,128]{1,0:T(8,128)(2,1)S(1)}, u32[]{:S(2)}, u32[]{:S(2)}) collective-permute-start(bf16[640,128]{1,0:T(8,128)(2,1)S(1)} %copy-done), channel_id=1, source_target_pairs={{0,16},{8,24},{16,0},{24,8},{1,17},{9,25},{17,1},{25,9},{2,18},{10... | collective-permute-start | bytes 491528 | tf_op jit(solution)/shard_map/ppermute | solution.py:35
  22.2 1.5 %collective-permute-start.3 = (bf16[640,128]{1,0:T(8,128)(2,1)S(1)}, bf16[640,128]{1,0:T(8,128)(2,1)S(1)}, u32[]{:S(2)}, u32[]{:S(2)}) collective-permute-start(bf16[640,128]{1,0:T(8,128)(2,1)S(1)} %copy-done), channel_id=1, source_target_pairs={{0,24},{8,0},{16,8},{24,16},{1,25},{9,1},{17,9},{25,17},{2,26},{10... | collective-permute-start | bytes 491528 | tf_op jit(solution)/shard_map/ppermute | solution.py:35
  23.6 6.5 %grad.2.kept = bf16[320,2048]{1,0:T(8,128)(2,1)} custom-call(s32[1]{0:T(128)} %bitcast.core, bf16[320,2048]{1,0:T(8,128)(2,1)} %bitcast.18, bf16[320,2048]{1,0:T(8,128)(2,1)} %bitcast.20, bf16[2048,2048]{1,0:T(8,128)(2,1)} %h.3, bf16[2048,2048]{1,0:T(8,128)(2,1)} %o.3), custom_call_target="tpu_custom_call" | custom-call | flops 2684354560 | bytes 11000000 | tf_op jit(solution)/shard_map/grad/pallas_call | solution.py:109
  30.1 6.6 %all-to-all-done = bf16[16,128,256]{2,1,0:T(8,128)(2,1)} async-done(((bf16[16,128,256]{2,1,0:T(8,128)(2,1)}), bf16[16,128,256]{2,1,0:T(8,128)(2,1)}, u32[]{:S(2)}, u32[]{:S(2)}) %all-to-all-start) | async-done | bytes 1048608 | tf_op jit(solution)/shard_map/all_to_all | solution.py:369
  36.7 0.0 collective-permute-start.2
  36.7 0.0 collective-permute-done.4
  36.7 4.4 %collective-permute-done.5 = bf16[640,128]{1,0:T(8,128)(2,1)S(1)} collective-permute-done((bf16[640,128]{1,0:T(8,128)(2,1)S(1)}, bf16[640,128]{1,0:T(8,128)(2,1)S(1)}, u32[]{:S(2)}, u32[]{:S(2)}) %collective-permute-start.5) | collective-permute-done | bytes 163872 | tf_op jit(solution)/shard_map/ppermute | solution.py:35
  41.1 1.2 %collective-permute-start.9 = (bf16[2,640,128]{2,1,0:T(8,128)(2,1)S(1)}, bf16[2,640,128]{2,1,0:T(8,128)(2,1)S(1)}, u32[]{:S(2)}, u32[]{:S(2)}) collective-permute-start(bf16[2,640,128]{2,1,0:T(8,128)(2,1)S(1)} %pad_maximum_fusion.2.old_0b), channel_id=1, source_target_pairs={{0,32},{32,64},{64,96},{96,0},{1,33},{33,65},{65,97},{97,1},{2,34}... | collective-permute-start | bytes 983048 | tf_op jit(solution)/shard_map/ppermute | solution.py:35
  42.3 0.0 collective-permute-done.3
  42.3 0.0 copy-start.1
  42.3 0.7 copy-done.1
  42.9 1.0 %pad_maximum_fusion.1.old_0a = bf16[2,640,128]{2,1,0:T(8,128)(2,1)S(1)} fusion(bf16[1,640,128]{2,1,0:T(8,128)(2,1)} %bitcast.25, bf16[1,640,128]{2,1,0:T(8,128)(2,1)} %bitcast.24), kind=kLoop, calls=%fused_computation.1 | loop fusion | flops 163840 | bytes 655360 | tf_op jit(solution)/shard_map/stack | solution.py:375
  44.0 0.0 collective-permute-done.came
  44.0 3.4 %project.1 = bf16[256,640]{1,0:T(8,128)(2,1)} custom-call(bf16[320,2048]{1,0:T(8,128)(2,1)} %grad.2.kept, bf16[320,2048]{1,0:T(8,128)(2,1)} %collective-permute-done.came, bf16[2048,256]{1,0:T(8,128)(2,1)} %bitcast.6.basis.basis_own), custom_call_target="tpu_custom_call" | custom-call | flops 671088640 | bytes 4000000 | tf_op jit(solution)/shard_map/project/pallas_call | solution.py:158
  47.4 4.6 %all-to-all-start.1 = ((bf16[16,16,640]{2,1,0:T(8,128)(2,1)}), bf16[16,16,640]{2,1,0:T(8,128)(2,1)S(1)}, u32[]{:S(2)}, u32[]{:S(2)}) async-start(bf16[16,16,640]{2,1,0:T(8,128)(2,1)} %bitcast.21), calls=%async_computation.1 | async-start | bytes 655360 | tf_op jit(solution)/shard_map/all_to_all | solution.py:388
  52.0 3.1 %collective-permute-start.6 = (bf16[2,640,128]{2,1,0:T(8,128)(2,1)S(1)}, bf16[2,640,128]{2,1,0:T(8,128)(2,1)S(1)}, u32[]{:S(2)}, u32[]{:S(2)}) collective-permute-start(bf16[2,640,128]{2,1,0:T(8,128)(2,1)S(1)} %pad_maximum_fusion.1.old_0a), channel_id=1, source_target_pairs={{0,96},{32,0},{64,32},{96,64},{1,97},{33,1},{65,33},{97,65},{2,98}... | collective-permute-start | bytes 983048 | tf_op jit(solution)/shard_map/ppermute | solution.py:35
  55.1 6.2 %all-to-all-done.1.arrived = bf16[16,16,640]{2,1,0:T(8,128)(2,1)S(1)} async-done(((bf16[16,16,640]{2,1,0:T(8,128)(2,1)}), bf16[16,16,640]{2,1,0:T(8,128)(2,1)S(1)}, u32[]{:S(2)}, u32[]{:S(2)}) %all-to-all-start.1) | async-done | bytes 327712 | tf_op jit(solution)/shard_map/all_to_all | solution.py:388
  61.3 0.8 collect.1
  62.1 0.0 collective-permute-start.1
  62.1 0.9 collective-permute-start.7
  62.9 6.7 %all-to-all-start.2 = ((f32[128,1,128]{2,1,0:T(1,128)}), f32[128,1,128]{2,1,0:T(1,128)S(1)}, u32[]{:S(2)}, u32[]{:S(2)}) async-start(f32[128,1,128]{2,1,0:T(1,128)} %get-tuple-element.27), calls=%async_computation.2 | async-start | bytes 131072 | tf_op jit(solution)/shard_map/all_to_all | solution.py:399
  69.6 0.0 collective-permute-done.9.old_3b
  69.6 1.1 %collective-permute-start.8 = (bf16[2,640,128]{2,1,0:T(8,128)(2,1)S(1)}, bf16[2,640,128]{2,1,0:T(8,128)(2,1)S(1)}, u32[]{:S(2)}, u32[]{:S(2)}) collective-permute-start(bf16[2,640,128]{2,1,0:T(8,128)(2,1)S(1)} %pad_maximum_fusion.1.old_0a), channel_id=1, source_target_pairs={{0,32},{32,64},{64,96},{96,0},{1,33},{33,65},{65,97},{97,1},{2,34}... | collective-permute-start | bytes 983048 | tf_op jit(solution)/shard_map/ppermute | solution.py:35
  70.8 0.0 collective-permute-done.6.old_1a
  70.8 1.7 %collective-permute-start.11 = (bf16[2,640,128]{2,1,0:T(8,128)(2,1)S(1)}, bf16[2,640,128]{2,1,0:T(8,128)(2,1)S(1)}, u32[]{:S(2)}, u32[]{:S(2)}) collective-permute-start(bf16[2,640,128]{2,1,0:T(8,128)(2,1)S(1)} %collective-permute-done.9.old_3b), channel_id=1, source_target_pairs={{0,32},{32,64},{64,96},{96,0},{1,33},{33,65},{65,97},{97,1},{2,34}... | collective-permute-start | bytes 983048 | tf_op jit(solution)/shard_map/ppermute | solution.py:35
  72.5 0.0 collective-permute-done.1.came
  72.5 1.5 %collective-permute-start.10 = (bf16[2,640,128]{2,1,0:T(8,128)(2,1)S(1)}, bf16[2,640,128]{2,1,0:T(8,128)(2,1)S(1)}, u32[]{:S(2)}, u32[]{:S(2)}) collective-permute-start(bf16[2,640,128]{2,1,0:T(8,128)(2,1)S(1)} %collective-permute-done.6.old_1a), channel_id=1, source_target_pairs={{0,96},{32,0},{64,32},{96,64},{1,97},{33,1},{65,33},{97,65},{2,98}... | collective-permute-start | bytes 983048 | tf_op jit(solution)/shard_map/ppermute | solution.py:35
  74.0 0.8 pad_maximum_fusion.4.old
  74.8 4.1 %all-to-all-done.2.totals = f32[128,1,128]{2,1,0:T(1,128)S(1)} async-done(((f32[128,1,128]{2,1,0:T(1,128)}), f32[128,1,128]{2,1,0:T(1,128)S(1)}, u32[]{:S(2)}, u32[]{:S(2)}) %all-to-all-start.2) | async-done | bytes 65568 | tf_op jit(solution)/shard_map/all_to_all | solution.py:399
  78.9 1.0 %apply.1 = (f32[16,320]{1,0:T(8,128)}, f32[16,320]{1,0:T(8,128)}, f32[16,320]{1,0:T(8,128)}, f32[16,320]{1,0:T(8,128)}, bf16[16,16,640]{2,1,0:T(8,128)(2,1)}) custom-call(s32[1]{0:T(128)} %bitcast.core, f32[128,1,128]{2,1,0:T(1,128)S(1)} %all-to-all-done.2.totals, f32[16,320]{1,0:T(8,128)S(1)} %get-tuple-element.28.kept, ...), custom_call_target="tpu_custom_call" | custom-call | flops 1000000 | bytes 500000 | tf_op jit(solution)/shard_map/apply/pallas_call | solution.py:232
  79.9 3.5 %all-to-all-start.3 = ((bf16[16,16,640]{2,1,0:T(8,128)(2,1)}), bf16[16,16,640]{2,1,0:T(8,128)(2,1)S(1)}, u32[]{:S(2)}, u32[]{:S(2)}) async-start(bf16[16,16,640]{2,1,0:T(8,128)(2,1)} %get-tuple-element.30), calls=%async_computation.3 | async-start | bytes 655360 | tf_op jit(solution)/shard_map/all_to_all | solution.py:404
  83.5 1.0 %pad_maximum_fusion.weights = f32[640,128]{1,0:T(8,128)S(1)} fusion(f32[320,128]{1,0:T(8,128)} %w_out.1, f32[320,128]{1,0:T(8,128)} %bitcast.23), kind=kLoop, calls=%fused_computation | loop fusion | flops 81920 | bytes 655360 | tf_op jit(solution)/shard_map/concatenate | solution.py:395
  84.5 0.9 pad_maximum_fusion.3.bases
  85.4 0.0 collective-permute-done.7.old_1b
  85.4 0.0 collective-permute-done.8.old_3a
  85.4 3.0 %collective-permute-done.11.old_2b = bf16[2,640,128]{2,1,0:T(8,128)(2,1)S(1)} collective-permute-done((bf16[2,640,128]{2,1,0:T(8,128)(2,1)S(1)}, bf16[2,640,128]{2,1,0:T(8,128)(2,1)S(1)}, u32[]{:S(2)}, u32[]{:S(2)}) %collective-permute-start.11) | collective-permute-done | bytes 327712 | tf_op jit(solution)/shard_map/ppermute | solution.py:35
  88.4 0.0 collective-permute-done.10.old_2a
  88.5 4.5 %all-to-all-done.3 = bf16[16,16,640]{2,1,0:T(8,128)(2,1)S(1)} async-done(((bf16[16,16,640]{2,1,0:T(8,128)(2,1)}), bf16[16,16,640]{2,1,0:T(8,128)(2,1)S(1)}, u32[]{:S(2)}, u32[]{:S(2)}) %all-to-all-start.3) | async-done | bytes 327712 | tf_op jit(solution)/shard_map/all_to_all | solution.py:404
  93.0 0.0 collective-permute-done.2.basis_other
  93.0 5.3 %final.1 = (f32[320,128]{1,0:T(8,128)}, f32[320,128]{1,0:T(8,128)}, bf16[320,2048]{1,0:T(8,128)(2,1)}, f32[320,128]{1,0:T(8,128)}, f32[320,128]{1,0:T(8,128)}, /*index=5*/bf16[320,2048]{1,0:T(8,128)(2,1)}) custom-call(s32[1]{0:T(128)} %bitcast.core, s32[1]{0:T(128)} %bitcast.1.at_x, s32[1]{0:T(128)} %bitcast.2.at_z, bf16[256,640]{1,0:T(8,128)(2,1)S(1)} %bitcast.16, ...), custom_call_target="tpu_custom_call" | custom-call | flops 700000000 | bytes 10000000 | tf_op jit(solution)/shard_map/final/pallas_call | solution.py:317
  (1 shorter events, 0.0 us)
Async XLA Ops:
  7.1 36.9 %collective-permute-start = (bf16[320,2048]{1,0:T(8,128)(2,1)}, bf16[320,2048]{1,0:T(8,128)(2,1)}, u32[]{:S(2)}, u32[]{:S(2)}) collective-permute-start(bf16[320,2048]{1,0:T(8,128)(2,1)} %grad.3), channel_id=1, source_target_pairs={{0,1},{1,0},{2,3},{3,2},{4,5},{5,4},{6,7},{7,6},{8,9},{9,8},{10,11... | collective-permute-start | bytes 3932168 | tf_op jit(solution)/shard_map/ppermute | solution.py:31
  9.4 8.2 %copy-start = (bf16[640,128]{1,0:T(8,128)(2,1)S(1)}, bf16[640,128]{1,0:T(8,128)(2,1)}, u32[]{:S(2)}) copy-start(bf16[640,128]{1,0:T(8,128)(2,1)} %get-tuple-element.31) | copy-start | bytes 491524
  9.4 27.3 %all-to-all-start = ((bf16[16,128,256]{2,1,0:T(8,128)(2,1)}), bf16[16,128,256]{2,1,0:T(8,128)(2,1)}, u32[]{:S(2)}, u32[]{:S(2)}) async-start(bf16[16,128,256]{2,1,0:T(8,128)(2,1)} %get-tuple-element.26), calls=%async_computation | async-start | bytes 2097152 | tf_op jit(solution)/shard_map/all_to_all | solution.py:369
  17.5 19.1 %collective-permute-start.4 = (bf16[640,128]{1,0:T(8,128)(2,1)S(1)}, bf16[640,128]{1,0:T(8,128)(2,1)S(1)}, u32[]{:S(2)}, u32[]{:S(2)}) collective-permute-start(bf16[640,128]{1,0:T(8,128)(2,1)S(1)} %copy-done), channel_id=1, source_target_pairs={{0,8},{8,16},{16,24},{24,0},{1,9},{9,17},{17,25},{25,1},{2,10},{10... | collective-permute-start | bytes 491528 | tf_op jit(solution)/shard_map/ppermute | solution.py:35
  19.5 21.6 %collective-permute-start.5 = (bf16[640,128]{1,0:T(8,128)(2,1)S(1)}, bf16[640,128]{1,0:T(8,128)(2,1)S(1)}, u32[]{:S(2)}, u32[]{:S(2)}) collective-permute-start(bf16[640,128]{1,0:T(8,128)(2,1)S(1)} %copy-done), channel_id=1, source_target_pairs={{0,16},{8,24},{16,0},{24,8},{1,17},{9,25},{17,1},{25,9},{2,18},{10... | collective-permute-start | bytes 491528 | tf_op jit(solution)/shard_map/ppermute | solution.py:35
  22.2 20.1 %collective-permute-start.3 = (bf16[640,128]{1,0:T(8,128)(2,1)S(1)}, bf16[640,128]{1,0:T(8,128)(2,1)S(1)}, u32[]{:S(2)}, u32[]{:S(2)}) collective-permute-start(bf16[640,128]{1,0:T(8,128)(2,1)S(1)} %copy-done), channel_id=1, source_target_pairs={{0,24},{8,0},{16,8},{24,16},{1,25},{9,1},{17,9},{25,17},{2,26},{10... | collective-permute-start | bytes 491528 | tf_op jit(solution)/shard_map/ppermute | solution.py:35
  36.7 56.3 %collective-permute-start.2 = (bf16[2048,256]{1,0:T(8,128)(2,1)}, bf16[2048,256]{1,0:T(8,128)(2,1)}, u32[]{:S(2)}, u32[]{:S(2)}) collective-permute-start(bf16[2048,256]{1,0:T(8,128)(2,1)} %bitcast.6.basis.basis_own), channel_id=1, source_target_pairs={{0,1},{1,0},{2,3},{3,2},{4,5},{5,4},{6,7},{7,6},{8,9},{9,8},{10,11... | collective-permute-start | bytes 3145736 | tf_op jit(solution)/shard_map/ppermute | solution.py:31
  41.1 28.5 %collective-permute-start.9 = (bf16[2,640,128]{2,1,0:T(8,128)(2,1)S(1)}, bf16[2,640,128]{2,1,0:T(8,128)(2,1)S(1)}, u32[]{:S(2)}, u32[]{:S(2)}) collective-permute-start(bf16[2,640,128]{2,1,0:T(8,128)(2,1)S(1)} %pad_maximum_fusion.2.old_0b), channel_id=1, source_target_pairs={{0,32},{32,64},{64,96},{96,0},{1,33},{33,65},{65,97},{97,1},{2,34}... | collective-permute-start | bytes 983048 | tf_op jit(solution)/shard_map/ppermute | solution.py:35
  42.3 0.7 copy-start.1
  47.4 13.9 %all-to-all-start.1 = ((bf16[16,16,640]{2,1,0:T(8,128)(2,1)}), bf16[16,16,640]{2,1,0:T(8,128)(2,1)S(1)}, u32[]{:S(2)}, u32[]{:S(2)}) async-start(bf16[16,16,640]{2,1,0:T(8,128)(2,1)} %bitcast.21), calls=%async_computation.1 | async-start | bytes 655360 | tf_op jit(solution)/shard_map/all_to_all | solution.py:388
  52.0 18.8 %collective-permute-start.6 = (bf16[2,640,128]{2,1,0:T(8,128)(2,1)S(1)}, bf16[2,640,128]{2,1,0:T(8,128)(2,1)S(1)}, u32[]{:S(2)}, u32[]{:S(2)}) collective-permute-start(bf16[2,640,128]{2,1,0:T(8,128)(2,1)S(1)} %pad_maximum_fusion.1.old_0a), channel_id=1, source_target_pairs={{0,96},{32,0},{64,32},{96,64},{1,97},{33,1},{65,33},{97,65},{2,98}... | collective-permute-start | bytes 983048 | tf_op jit(solution)/shard_map/ppermute | solution.py:35
  62.1 10.4 %collective-permute-start.1 = (f32[16,320]{1,0:T(8,128)S(1)}, f32[16,320]{1,0:T(8,128)S(1)}, u32[]{:S(2)}, u32[]{:S(2)}) collective-permute-start(f32[16,320]{1,0:T(8,128)S(1)} %get-tuple-element.29), channel_id=1, source_target_pairs={{0,1},{1,0},{2,3},{3,2},{4,5},{5,4},{6,7},{7,6},{8,9},{9,8},{10,11... | collective-permute-start | bytes 61448 | tf_op jit(solution)/shard_map/ppermute | solution.py:31
  62.1 23.3 %collective-permute-start.7 = (bf16[2,640,128]{2,1,0:T(8,128)(2,1)S(1)}, bf16[2,640,128]{2,1,0:T(8,128)(2,1)S(1)}, u32[]{:S(2)}, u32[]{:S(2)}) collective-permute-start(bf16[2,640,128]{2,1,0:T(8,128)(2,1)S(1)} %pad_maximum_fusion.2.old_0b), channel_id=1, source_target_pairs={{0,96},{32,0},{64,32},{96,64},{1,97},{33,1},{65,33},{97,65},{2,98}... | collective-permute-start | bytes 983048 | tf_op jit(solution)/shard_map/ppermute | solution.py:35
  62.9 16.0 %all-to-all-start.2 = ((f32[128,1,128]{2,1,0:T(1,128)}), f32[128,1,128]{2,1,0:T(1,128)S(1)}, u32[]{:S(2)}, u32[]{:S(2)}) async-start(f32[128,1,128]{2,1,0:T(1,128)} %get-tuple-element.27), calls=%async_computation.2 | async-start | bytes 131072 | tf_op jit(solution)/shard_map/all_to_all | solution.py:399
  69.6 15.8 %collective-permute-start.8 = (bf16[2,640,128]{2,1,0:T(8,128)(2,1)S(1)}, bf16[2,640,128]{2,1,0:T(8,128)(2,1)S(1)}, u32[]{:S(2)}, u32[]{:S(2)}) collective-permute-start(bf16[2,640,128]{2,1,0:T(8,128)(2,1)S(1)} %pad_maximum_fusion.1.old_0a), channel_id=1, source_target_pairs={{0,32},{32,64},{64,96},{96,0},{1,33},{33,65},{65,97},{97,1},{2,34}... | collective-permute-start | bytes 983048 | tf_op jit(solution)/shard_map/ppermute | solution.py:35
  70.8 17.7 %collective-permute-start.11 = (bf16[2,640,128]{2,1,0:T(8,128)(2,1)S(1)}, bf16[2,640,128]{2,1,0:T(8,128)(2,1)S(1)}, u32[]{:S(2)}, u32[]{:S(2)}) collective-permute-start(bf16[2,640,128]{2,1,0:T(8,128)(2,1)S(1)} %collective-permute-done.9.old_3b), channel_id=1, source_target_pairs={{0,32},{32,64},{64,96},{96,0},{1,33},{33,65},{65,97},{97,1},{2,34}... | collective-permute-start | bytes 983048 | tf_op jit(solution)/shard_map/ppermute | solution.py:35
  72.5 15.9 %collective-permute-start.10 = (bf16[2,640,128]{2,1,0:T(8,128)(2,1)S(1)}, bf16[2,640,128]{2,1,0:T(8,128)(2,1)S(1)}, u32[]{:S(2)}, u32[]{:S(2)}) collective-permute-start(bf16[2,640,128]{2,1,0:T(8,128)(2,1)S(1)} %collective-permute-done.6.old_1a), channel_id=1, source_target_pairs={{0,96},{32,0},{64,32},{96,64},{1,97},{33,1},{65,33},{97,65},{2,98}... | collective-permute-start | bytes 983048 | tf_op jit(solution)/shard_map/ppermute | solution.py:35
  79.9 13.1 %all-to-all-start.3 = ((bf16[16,16,640]{2,1,0:T(8,128)(2,1)}), bf16[16,16,640]{2,1,0:T(8,128)(2,1)S(1)}, u32[]{:S(2)}, u32[]{:S(2)}) async-start(bf16[16,16,640]{2,1,0:T(8,128)(2,1)} %get-tuple-element.30), calls=%async_computation.3 | async-start | bytes 655360 | tf_op jit(solution)/shard_map/all_to_all | solution.py:404

commit v2 on v1

--- a/solution.py
+++ b/solution.py
@@ -1,4 +1,3 @@
-import functools
 import math
 
 import jax
@@ -39,7 +38,7 @@
     return lax.dot_general(a, b, (dims, ((), ())), preferred_element_type=F32)
 
 
-def pack_kernel(core, w_in, w_out, b_in, b_out, weights, bases):
+def pack_kernel(core, at_x, at_z, w_in, w_out, b_in, b_out, weights, bases):
     weights[0:W, :] = w_in[...].astype(BF16)
     weights[W : 2 * W, :] = w_out[...].astype(BF16)
     mine = jnp.where(core[0] == 0, b_in[...], b_out[...])
@@ -56,6 +55,8 @@
         ),
         grid=(1,),
         in_specs=[
+            SMEM,
+            SMEM,
             SMEM,
             pl.BlockSpec((W, 128), lambda i: (0, 0)),
             pl.BlockSpec((W, 128), lambda i: (0, 0)),
@@ -75,29 +76,32 @@
 GRAD_TILES = 2048 // GRAD_TILE
 
 
-def grad_kernel(flip, core, conv, lru, h, o, out, wide, tall, sems):
-    uses_in = core[0] == flip
-
+def grad_kernel(core, conv, conv_came, lru, lru_came, h, o, out, wide, tall, sems):
     def tile(source, k):
         cols = slice(k * GRAD_TILE, (k + 1) * GRAD_TILE)
         return pltpu.make_async_copy(source.at[:, cols], tall.at[k], sems.at[k])
 
-    def factor(source):
-        return pltpu.make_async_copy(source, wide, sems.at[GRAD_TILES])
-
-    @pl.when(uses_in)
+    def half(source, k):
+        return pltpu.make_async_copy(
+            source, wide.at[k * W : (k + 1) * W], sems.at[GRAD_TILES + k]
+        )
+
+    def start(own, came, source):
+        half(own, 0).start()
+        half(came, 1).start()
+        for k in range(GRAD_TILES):
+            tile(source, k).start()
+
+    @pl.when(core[0] == 0)
     def _():
-        factor(conv).start()
-        for k in range(GRAD_TILES):
-            tile(h, k).start()
-
-    @pl.when(jnp.logical_not(uses_in))
+        start(conv, conv_came, h)
+
+    @pl.when(core[0] != 0)
     def _():
-        factor(lru).start()
-        for k in range(GRAD_TILES):
-            tile(o, k).start()
-
-    factor(conv).wait()
+        start(lru, lru_came, o)
+
+    half(conv, 0).wait()
+    half(conv_came, 1).wait()
     for k in range(GRAD_TILES):
         tile(h, k).wait()
         out[:, k * GRAD_TILE : (k + 1) * GRAD_TILE] = jnp.dot(
@@ -105,29 +109,29 @@
         ).astype(BF16)
 
 
-def grad(flip, core, conv, lru, h, o):
-    return pl.pallas_call(
-        functools.partial(grad_kernel, flip),
-        in_specs=[SMEM] + [pl.BlockSpec(memory_space=pltpu.HBM)] * 4,
+def grad(*args):
+    return pl.pallas_call(
+        grad_kernel,
+        in_specs=[SMEM] + [pl.BlockSpec(memory_space=pltpu.HBM)] * 6,
         out_specs=VMEM,
-        out_shape=jax.ShapeDtypeStruct((W, 2048), BF16),
+        out_shape=jax.ShapeDtypeStruct((2 * W, 2048), BF16),
         scratch_shapes=[
-            pltpu.VMEM((W, 2048), BF16),
+            pltpu.VMEM((2 * W, 2048), BF16),
             pltpu.VMEM((GRAD_TILES, 2048, GRAD_TILE), BF16),
-            pltpu.SemaphoreType.DMA((GRAD_TILES + 1,)),
+            pltpu.SemaphoreType.DMA((GRAD_TILES + 2,)),
         ],
         name="grad",
         compiler_params=pltpu.CompilerParams(vmem_limit_bytes=63 << 20),
         cost_estimate=pl.CostEstimate(
-            flops=2 * 2048 * 2048 * W, bytes_accessed=11_000_000, transcendentals=0
-        ),
-    )(core, conv, lru, h, o)
+            flops=4 * 2048 * 2048 * W, bytes_accessed=14_000_000, transcendentals=0
+        ),
+    )(*args)
 
 
 PROJECT_TILES = 4
 
 
-def project_kernel(kept, came, basis, out, kept_in, came_in, basis_in, sems):
+def project_kernel(grads, basis, out, grads_in, basis_in, sems):
     depth = 2048 // PROJECT_TILES
     copies = []
     for k in range(PROJECT_TILES):
@@ -135,8 +139,7 @@
         copies.append(
             (
                 pltpu.make_async_copy(basis.at[at], basis_in.at[k], sems.at[0, k]),
-                pltpu.make_async_copy(kept.at[:, at], kept_in.at[k], sems.at[1, k]),
-                pltpu.make_async_copy(came.at[:, at], came_in.at[k], sems.at[2, k]),
+                pltpu.make_async_copy(grads.at[:, at], grads_in.at[k], sems.at[1, k]),
             )
         )
     for group in copies:
@@ -147,31 +150,30 @@
     for k in range(PROJECT_TILES):
         for copy in copies[k]:
             copy.wait()
-        mine = mine + jnp.dot(kept_in[k], basis_in[k], preferred_element_type=F32)
-        other = other + jnp.dot(came_in[k], basis_in[k], preferred_element_type=F32)
+        mine = mine + jnp.dot(grads_in[k, 0:W], basis_in[k], preferred_element_type=F32)
+        other = other + jnp.dot(grads_in[k, W:], basis_in[k], preferred_element_type=F32)
     out[:, 0:W] = mine.T.astype(BF16)
     out[:, W:] = other.T.astype(BF16)
 
 
-def project(kept, came, basis):
+def project(grads, basis):
     depth = 2048 // PROJECT_TILES
     return pl.pallas_call(
         project_kernel,
-        in_specs=[pl.BlockSpec(memory_space=pltpu.HBM)] * 3,
+        in_specs=[pl.BlockSpec(memory_space=pltpu.HBM)] * 2,
         out_specs=VMEM,
         out_shape=jax.ShapeDtypeStruct((RANK, 2 * W), BF16),
         scratch_shapes=[
-            pltpu.VMEM((PROJECT_TILES, W, depth), BF16),
-            pltpu.VMEM((PROJECT_TILES, W, depth), BF16),
+            pltpu.VMEM((PROJECT_TILES, 2 * W, depth), BF16),
             pltpu.VMEM((PROJECT_TILES, depth, RANK), BF16),
-            pltpu.SemaphoreType.DMA((3, PROJECT_TILES)),
+            pltpu.SemaphoreType.DMA((2, PROJECT_TILES)),
         ],
         name="project",
         compiler_params=pltpu.CompilerParams(vmem_limit_bytes=63 << 20),
         cost_estimate=pl.CostEstimate(
             flops=4 * 2048 * RANK * W, bytes_accessed=4_000_000, transcendentals=0
         ),
-    )(kept, came, basis)
+    )(grads, basis)
 
 
 def collect_kernel(arrived, kept, given, squares):
@@ -249,6 +251,7 @@
     at_x,
     at_z,
     full,
+    mark,
     bases,
     weights,
     basis_own,
@@ -302,7 +305,7 @@
             write(lambda r: jnp.where(r < 2, near[r & 1], far[r & 1]))
 
 
-def final(core, at_x, at_z, full, bases, weights, own, other, old):
+def final(core, at_x, at_z, full, mark, bases, weights, own, other, old):
     shape = jax.ShapeDtypeStruct
 
     def whole(s):
@@ -321,6 +324,7 @@
             grid=(SIDE,),
             in_specs=[
                 whole((RANK, 2 * W)),
+                whole((8, 128)),
                 whole((2 * 128, RANK)),
                 whole((2 * W, 128)),
                 tile,
@@ -343,7 +347,7 @@
         cost_estimate=pl.CostEstimate(
             flops=700_000_000, bytes_accessed=10_000_000, transcendentals=0
         ),
-    )(core, at_x, at_z, full, bases, weights, own, other, *old)
+    )(core, at_x, at_z, full, mark, bases, weights, own, other, *old)
 
 
 def shards(
@@ -364,7 +368,7 @@
     at_z = lax.axis_index("fs_0").astype(jnp.int32).reshape(1)
     at_x = lax.axis_index("fs_1").astype(jnp.int32).reshape(1)
 
-    packed, bases = pack(core, weight_in.T, weight_out, basis_in, basis_out)
+    packed, bases = pack(core, at_x, at_z, weight_in.T, weight_out, basis_in, basis_out)
 
     basis_own = lax.all_to_all(bases, FS, 0, 0, tiled=True).reshape(-1, RANK)
     basis_other = swapped(basis_own)
@@ -372,6 +376,10 @@
     pieces = [packed]
     for d in (1, 3, 2):
         pieces.append(shifted(packed, "fs_1", -d))
+    old_weights = lax.optimization_barrier(
+        jnp.concatenate((weight_in.T, weight_out), axis=0)
+    )
+    pieces[0] = old_weights.astype(BF16)
     halves = [lax.optimization_barrier(jnp.stack(pieces[k : k + 2])) for k in (0, 2)]
     old = list(halves)
     for d in (1, 3):
@@ -380,19 +388,16 @@
     old.append(shifted(old[2], "fs_0", -1))
     old.append(shifted(old[5], "fs_0", -3))
 
-    wide = (conv_cotan.T, lru_out.T, h_saved, out_cotan)
-    given = grad(1, core, *wide)
-    came = swapped(given)
-    kept = grad(0, core, *wide)
-    part = project(kept, came, basis_own)
+    conv, lru = conv_cotan.T, lru_out.T
+    conv_came = swapped(conv)
+    lru_came = swapped(lru)
+    grads = grad(core, conv, conv_came, lru, lru_came, h_saved, out_cotan)
+    part = project(grads, basis_own)
     arrived = lax.all_to_all(
         part.reshape(PEERS, ROWS, 2 * W), FS, split_axis=0, concat_axis=0, tiled=True
     )
     old_moments = lax.optimization_barrier(
         jnp.concatenate((first_in, second_in, first_out, second_out), axis=0)
-    )
-    old_weights = lax.optimization_barrier(
-        jnp.concatenate((weight_in.T, weight_out), axis=0)
     )
     own_bases = lax.optimization_barrier(jnp.concatenate((basis_in, basis_out), axis=0))
     proj_own, proj_given, squares = collect(arrived)
@@ -402,8 +407,9 @@
         core, totals, proj_own, proj_other, old_moments
     )
     full = lax.all_to_all(dirs, FS, 0, 0, tiled=True).reshape(RANK, 2 * W)
+    mark = lax.optimization_barrier(full[:8, :128])
     step_in, new_in, copy_in, step_out, new_out, copy_out = final(
-        core, at_x, at_z, full, own_bases, old_weights, basis_own, basis_other, old
+        core, at_x, at_z, full, mark, own_bases, old_weights, basis_own, basis_other, old
     )
     return (
         step_in.T,

time: 99 us -> 102 us (1.030)
  waiting for transfers between devices: 28.8 us -> 36.6 us
  other arithmetic: 3.76 us -> 0.92 us
  Pallas kernels: 25.6 us -> 22.8 us
  starting transfers between devices: 38.7 us -> 39.9 us
    ppermute x9, waiting for transfers between devices: 7.48 us -> 16.1 us  [shifted(): lax.ppermute(array, axis, [(i, (i + by) % SIDE) for i in range(SIDE)])]
    all_to_all x1, waiting for transfers between devices: 6.58 us -> 0.01 us  [shards(): basis_own = lax.all_to_all(bases, FS, 0, 0, tiled=True).reshape(-1, RANK)]
    all_to_all x1, waiting for transfers between devices: 4.54 us -> 9.49 us  [shards(): full = lax.all_to_all(dirs, FS, 0, 0, tiled=True).reshape(RANK, 2 * W)]
    pallas_call x2 -> x1, Pallas kernels: 12.9 us -> 10 us  [grad(): pl.pallas_call(grad_kernel, in_specs=[SMEM] + [pl.BlockSpec(memory_space=...]
  transfers between devices with their start and end apart: 16 -> 17, of which waited for: 6 -> 5; matrix products, arithmetic and copies ran while one was open for 4% -> 1% of each run, Pallas kernels for 14% -> 17%
where the time goes in v2:
time: 102 us; the launch traced here: 101 us
  starting transfers between devices  39.9 us (39%)
  waiting for transfers between devices  36.6 us (36%)
  Pallas kernels  22.8 us (22%)
    ppermute x9, waiting for transfers between devices, shifted(): lax.ppermute(array, axis, [(i, (i + by) % SIDE) for i in range(SIDE)])  16.1 us
    ppermute x9, starting transfers between devices, shifted(): lax.ppermute(array, axis, [(i, (i + by) % SIDE) for i in range(SIDE)])  16 us
    pallas_call x1, Pallas kernels, grad(): pl.pallas_call(grad_kernel, in_specs=[SMEM] + [pl.BlockSpec(memory_space=...  10 us
    all_to_all x1, waiting for transfers between devices, shards(): full = lax.all_to_all(dirs, FS, 0, 0, tiled=True).reshape(RANK, 2 * W)  9.49 us
    all_to_all x1, starting transfers between devices, shards(): basis_own = lax.all_to_all(bases, FS, 0, 0, tiled=True).reshape(-1, RANK)  8.17 us
    all_to_all x1, waiting for transfers between devices, shards(): lax.all_to_all(part.reshape(PEERS, ROWS, 2 * W), FS, split_axis=0, concat...  6.88 us
    all_to_all x1, starting transfers between devices, shards(): totals = lax.all_to_all(squares, EVERY, 0, 0, tiled=True)  6.64 us
    pallas_call x1, Pallas kernels, final(): pl.pallas_call(final_kernel, grid_spec=pltpu.PrefetchScalarGridSpec(num_s...  5.44 us
  transfers between devices with their start and end apart: 17, of which 5 were waited for; matrix products, arithmetic and copies ran while one was open for 1% of the time, Pallas kernels for 17%

profile of v2, /device:TPU:0, one launch (start us, length us, event | category | flops | bytes accessed | tf_op | source)
XLA Modules:
  0.0 101.1 jit_solution(2719264547528684790)
XLA Ops:
  0.6 0.0 copy-start
  0.7 0.0 copy-start.1
  0.7 0.1 collective-permute-start
  0.8 0.5 collective-permute-start.1
  1.3 2.1 %pack.1 = (bf16[640,128]{1,0:T(8,128)(2,1)}, bf16[16,128,256]{2,1,0:T(8,128)(2,1)}) custom-call(s32[1]{0:T(128)} %bitcast.core, s32[1]{0:T(128)} %bitcast.1.at_x, s32[1]{0:T(128)} %bitcast.2.at_z, f32[320,128]{1,0:T(8,128)} %bitcast.24, f32[320,128]{1,0:T(8,128)} %w_out.1, bf16[128,256]{1,0:T(8,128)(2,1)} %b_in.1, bf16[128,256]{1,0:T(8,128)(2,1)} %b_out.1), custom_call_target="tpu_custom_call" | custom-call | flops 1000000 | bytes 500000 | tf_op jit(solution)/shard_map/pack/pallas_call | solution.py:50
  3.4 0.0 copy-start.4
  3.4 8.2 %all-to-all-start = ((bf16[16,128,256]{2,1,0:T(8,128)(2,1)}), bf16[16,128,256]{2,1,0:T(8,128)(2,1)}, u32[]{:S(2)}, u32[]{:S(2)}) async-start(bf16[16,128,256]{2,1,0:T(8,128)(2,1)} %get-tuple-element.26), calls=%async_computation | async-start | bytes 2097152 | tf_op jit(solution)/shard_map/all_to_all | solution.py:373
  11.6 0.0 copy-done.4
  11.6 1.9 %collective-permute-start.5 = (bf16[640,128]{1,0:T(8,128)(2,1)S(1)}, bf16[640,128]{1,0:T(8,128)(2,1)S(1)}, u32[]{:S(2)}, u32[]{:S(2)}) collective-permute-start(bf16[640,128]{1,0:T(8,128)(2,1)S(1)} %copy-done.4), channel_id=1, source_target_pairs={{0,8},{8,16},{16,24},{24,0},{1,9},{9,17},{17,25},{25,1},{2,10},{10... | collective-permute-start | bytes 491528 | tf_op jit(solution)/shard_map/ppermute | solution.py:34
  13.5 2.7 %collective-permute-start.6 = (bf16[640,128]{1,0:T(8,128)(2,1)S(1)}, bf16[640,128]{1,0:T(8,128)(2,1)S(1)}, u32[]{:S(2)}, u32[]{:S(2)}) collective-permute-start(bf16[640,128]{1,0:T(8,128)(2,1)S(1)} %copy-done.4), channel_id=1, source_target_pairs={{0,16},{8,24},{16,0},{24,8},{1,17},{9,25},{17,1},{25,9},{2,18},{10... | collective-permute-start | bytes 491528 | tf_op jit(solution)/shard_map/ppermute | solution.py:34
  16.2 1.5 %collective-permute-start.4 = (bf16[640,128]{1,0:T(8,128)(2,1)S(1)}, bf16[640,128]{1,0:T(8,128)(2,1)S(1)}, u32[]{:S(2)}, u32[]{:S(2)}) collective-permute-start(bf16[640,128]{1,0:T(8,128)(2,1)S(1)} %copy-done.4), channel_id=1, source_target_pairs={{0,24},{8,0},{16,8},{24,16},{1,25},{9,1},{17,9},{25,17},{2,26},{10... | collective-permute-start | bytes 491528 | tf_op jit(solution)/shard_map/ppermute | solution.py:34
  17.6 0.0 copy-done
  17.6 0.0 copy-done.1
  17.7 13.1 %collective-permute-done.5 = bf16[640,128]{1,0:T(8,128)(2,1)S(1)} collective-permute-done((bf16[640,128]{1,0:T(8,128)(2,1)S(1)}, bf16[640,128]{1,0:T(8,128)(2,1)S(1)}, u32[]{:S(2)}, u32[]{:S(2)}) %collective-permute-start.5) | collective-permute-done | bytes 163872 | tf_op jit(solution)/shard_map/ppermute | solution.py:34
  30.7 3.1 %collective-permute-done.6 = bf16[640,128]{1,0:T(8,128)(2,1)S(1)} collective-permute-done((bf16[640,128]{1,0:T(8,128)(2,1)S(1)}, bf16[640,128]{1,0:T(8,128)(2,1)S(1)}, u32[]{:S(2)}, u32[]{:S(2)}) %collective-permute-start.6) | collective-permute-done | bytes 163872 | tf_op jit(solution)/shard_map/ppermute | solution.py:34
  33.9 1.5 %collective-permute-start.10 = (bf16[2,640,128]{2,1,0:T(8,128)(2,1)S(1)}, bf16[2,640,128]{2,1,0:T(8,128)(2,1)}, u32[]{:S(2)}, u32[]{:S(2)}) collective-permute-start(bf16[2,640,128]{2,1,0:T(8,128)(2,1)S(1)} %pad_maximum_fusion.2.old_0b), channel_id=1, source_target_pairs={{0,32},{32,64},{64,96},{96,0},{1,33},{33,65},{65,97},{97,1},{2,34}... | collective-permute-start | bytes 983048 | tf_op jit(solution)/shard_map/ppermute | solution.py:34
  35.4 0.0 collective-permute-done.4
  35.4 0.0 all-to-all-done
  35.4 0.1 collective-permute-start.3
  35.5 0.0 collective-permute-done.conv_came
  35.5 0.0 collective-permute-done.1.lru_came
  35.6 10.0 %grad.1.grads = bf16[640,2048]{1,0:T(8,128)(2,1)} custom-call(s32[1]{0:T(128)} %bitcast.core, bf16[320,2048]{1,0:T(8,128)(2,1)} %bitcast.21, bf16[320,2048]{1,0:T(8,128)(2,1)} %collective-permute-done.conv_came, bf16[320,2048]{1,0:T(8,128)(2,1)} %bitcast.23, bf16[320,2048]{1,0:T(8,128)(2,1)} %collective-permute-done.1.lru_came, bf16[2048,2048]{1,0:T(8,128)(2,1)} %h.1, ...), custom_call_target="tpu_custom_call" | custom-call | flops 5368709120 | bytes 14000000 | tf_op jit(solution)/shard_map/grad/pallas_call | solution.py:113
  45.6 3.4 %project.1 = bf16[256,640]{1,0:T(8,128)(2,1)} custom-call(bf16[640,2048]{1,0:T(8,128)(2,1)} %grad.1.grads, bf16[2048,256]{1,0:T(8,128)(2,1)} %bitcast.6.basis.basis_own), custom_call_target="tpu_custom_call" | custom-call | flops 671088640 | bytes 4000000 | tf_op jit(solution)/shard_map/project/pallas_call | solution.py:161
  49.0 0.0 copy-start.2
  49.0 0.0 copy-start.3
  49.0 4.9 %all-to-all-start.1 = ((bf16[16,16,640]{2,1,0:T(8,128)(2,1)}), bf16[16,16,640]{2,1,0:T(8,128)(2,1)S(1)}, u32[]{:S(2)}, u32[]{:S(2)}) async-start(bf16[16,16,640]{2,1,0:T(8,128)(2,1)} %bitcast.19), calls=%async_computation.1 | async-start | bytes 655360 | tf_op jit(solution)/shard_map/all_to_all | solution.py:396
  53.9 3.1 %collective-permute-start.7 = (bf16[2,640,128]{2,1,0:T(8,128)(2,1)S(1)}, bf16[2,640,128]{2,1,0:T(8,128)(2,1)S(1)}, u32[]{:S(2)}, u32[]{:S(2)}) collective-permute-start(bf16[2,640,128]{2,1,0:T(8,128)(2,1)S(1)} %pad_maximum_fusion.1.old_0a), channel_id=1, source_target_pairs={{0,96},{32,0},{64,32},{96,64},{1,97},{33,1},{65,33},{97,65},{2,98}... | collective-permute-start | bytes 983048 | tf_op jit(solution)/shard_map/ppermute | solution.py:34
  57.1 6.9 %all-to-all-done.1.arrived = bf16[16,16,640]{2,1,0:T(8,128)(2,1)S(1)} async-done(((bf16[16,16,640]{2,1,0:T(8,128)(2,1)}), bf16[16,16,640]{2,1,0:T(8,128)(2,1)S(1)}, u32[]{:S(2)}, u32[]{:S(2)}) %all-to-all-start.1) | async-done | bytes 327712 | tf_op jit(solution)/shard_map/all_to_all | solution.py:396
  63.9 0.8 collect.1
  64.7 0.0 collective-permute-start.2
  64.7 0.9 collective-permute-start.8
  65.6 6.6 %all-to-all-start.2 = ((f32[128,1,128]{2,1,0:T(1,128)}), f32[128,1,128]{2,1,0:T(1,128)S(1)}, u32[]{:S(2)}, u32[]{:S(2)}) async-start(f32[128,1,128]{2,1,0:T(1,128)} %get-tuple-element.27), calls=%async_computation.2 | async-start | bytes 131072 | tf_op jit(solution)/shard_map/all_to_all | solution.py:404
  72.2 0.0 collective-permute-done.10.old_3b
  72.2 1.1 %collective-permute-start.9 = (bf16[2,640,128]{2,1,0:T(8,128)(2,1)S(1)}, bf16[2,640,128]{2,1,0:T(8,128)(2,1)S(1)}, u32[]{:S(2)}, u32[]{:S(2)}) collective-permute-start(bf16[2,640,128]{2,1,0:T(8,128)(2,1)S(1)} %pad_maximum_fusion.1.old_0a), channel_id=1, source_target_pairs={{0,32},{32,64},{64,96},{96,0},{1,33},{33,65},{65,97},{97,1},{2,34}... | collective-permute-start | bytes 983048 | tf_op jit(solution)/shard_map/ppermute | solution.py:34
  73.4 0.0 collective-permute-done.7.old_1a
  73.4 1.7 %collective-permute-start.12 = (bf16[2,640,128]{2,1,0:T(8,128)(2,1)}, bf16[2,640,128]{2,1,0:T(8,128)(2,1)S(1)}, u32[]{:S(2)}, u32[]{:S(2)}) collective-permute-start(bf16[2,640,128]{2,1,0:T(8,128)(2,1)} %collective-permute-done.10.old_3b), channel_id=1, source_target_pairs={{0,32},{32,64},{64,96},{96,0},{1,33},{33,65},{65,97},{97,1},{2,34}... | collective-permute-start | bytes 983048 | tf_op jit(solution)/shard_map/ppermute | solution.py:34
  75.1 0.0 collective-permute-done.2.came
  75.1 1.5 %collective-permute-start.11 = (bf16[2,640,128]{2,1,0:T(8,128)(2,1)S(1)}, bf16[2,640,128]{2,1,0:T(8,128)(2,1)S(1)}, u32[]{:S(2)}, u32[]{:S(2)}) collective-permute-start(bf16[2,640,128]{2,1,0:T(8,128)(2,1)S(1)} %collective-permute-done.7.old_1a), channel_id=1, source_target_pairs={{0,96},{32,0},{64,32},{96,64},{1,97},{33,1},{65,33},{97,65},{2,98}... | collective-permute-start | bytes 983048 | tf_op jit(solution)/shard_map/ppermute | solution.py:34
  76.6 0.8 pad_maximum_fusion.4.old
  77.4 4.1 %all-to-all-done.2.totals = f32[128,1,128]{2,1,0:T(1,128)S(1)} async-done(((f32[128,1,128]{2,1,0:T(1,128)}), f32[128,1,128]{2,1,0:T(1,128)S(1)}, u32[]{:S(2)}, u32[]{:S(2)}) %all-to-all-start.2) | async-done | bytes 65568 | tf_op jit(solution)/shard_map/all_to_all | solution.py:404
  81.5 1.0 %apply.1 = (f32[16,320]{1,0:T(8,128)}, f32[16,320]{1,0:T(8,128)}, f32[16,320]{1,0:T(8,128)}, f32[16,320]{1,0:T(8,128)}, bf16[16,16,640]{2,1,0:T(8,128)(2,1)}) custom-call(s32[1]{0:T(128)} %bitcast.core, f32[128,1,128]{2,1,0:T(1,128)S(1)} %all-to-all-done.2.totals, f32[16,320]{1,0:T(8,128)S(1)} %get-tuple-element.28.kept, ...), custom_call_target="tpu_custom_call" | custom-call | flops 1000000 | bytes 500000 | tf_op jit(solution)/shard_map/apply/pallas_call | solution.py:234
  82.5 3.5 %all-to-all-start.3 = ((bf16[16,16,640]{2,1,0:T(8,128)(2,1)}), bf16[16,16,640]{2,1,0:T(8,128)(2,1)S(1)}, u32[]{:S(2)}, u32[]{:S(2)}) async-start(bf16[16,16,640]{2,1,0:T(8,128)(2,1)} %get-tuple-element.30), calls=%async_computation.3 | async-start | bytes 655360 | tf_op jit(solution)/shard_map/all_to_all | solution.py:409
  86.1 0.0 copy-done.2
  86.1 0.0 copy-done.3
  86.1 9.5 %all-to-all-done.3 = bf16[16,16,640]{2,1,0:T(8,128)(2,1)S(1)} async-done(((bf16[16,16,640]{2,1,0:T(8,128)(2,1)}), bf16[16,16,640]{2,1,0:T(8,128)(2,1)S(1)}, u32[]{:S(2)}, u32[]{:S(2)}) %all-to-all-start.3) | async-done | bytes 327712 | tf_op jit(solution)/shard_map/all_to_all | solution.py:409
  95.6 0.0 collective-permute-done.8.old_1b
  95.6 0.0 collective-permute-done.9.old_3a
  95.6 0.0 collective-permute-done.12.old_2b
  95.6 0.0 collective-permute-done.11.old_2a
  95.6 0.0 collective-permute-done.3.basis_other
  95.6 5.4 %final.1 = (f32[320,128]{1,0:T(8,128)}, f32[320,128]{1,0:T(8,128)}, bf16[320,2048]{1,0:T(8,128)(2,1)}, f32[320,128]{1,0:T(8,128)}, f32[320,128]{1,0:T(8,128)}, /*index=5*/bf16[320,2048]{1,0:T(8,128)(2,1)}) custom-call(s32[1]{0:T(128)} %bitcast.core, s32[1]{0:T(128)} %bitcast.1.at_x, s32[1]{0:T(128)} %bitcast.2.at_z, bf16[256,640]{1,0:T(8,128)(2,1)S(1)} %bitcast.18, ...), custom_call_target="tpu_custom_call" | custom-call | flops 700000000 | bytes 10000000 | tf_op jit(solution)/shard_map/final/pallas_call | solution.py:320
  (6 shorter events, 0.1 us)
Async XLA Ops:
  0.6 17.0 %copy-start = (f32[128,320]{0,1:T(8,128)S(1)}, f32[128,320]{0,1:T(8,128)}, u32[]{:S(2)}) copy-start(f32[128,320]{0,1:T(8,128)} %param.18) | copy-start | bytes 491524
  0.7 17.0 %copy-start.1 = (f32[320,128]{1,0:T(8,128)S(1)}, f32[320,128]{1,0:T(8,128)}, u32[]{:S(2)}) copy-start(f32[320,128]{1,0:T(8,128)} %w_out.1) | copy-start | bytes 491524
  0.7 34.9 %collective-permute-start = (bf16[320,2048]{1,0:T(8,128)(2,1)}, bf16[320,2048]{1,0:T(8,128)(2,1)}, u32[]{:S(2)}, u32[]{:S(2)}) collective-permute-start(bf16[320,2048]{1,0:T(8,128)(2,1)} %bitcast.20), channel_id=1, source_target_pairs={{0,1},{1,0},{2,3},{3,2},{4,5},{5,4},{6,7},{7,6},{8,9},{9,8},{10,11... | collective-permute-start | bytes 3932168 | tf_op jit(solution)/shard_map/ppermute | solution.py:30
  0.8 34.8 %collective-permute-start.1 = (bf16[320,2048]{1,0:T(8,128)(2,1)}, bf16[320,2048]{1,0:T(8,128)(2,1)}, u32[]{:S(2)}, u32[]{:S(2)}) collective-permute-start(bf16[320,2048]{1,0:T(8,128)(2,1)} %bitcast.22), channel_id=1, source_target_pairs={{0,1},{1,0},{2,3},{3,2},{4,5},{5,4},{6,7},{7,6},{8,9},{9,8},{10,11... | collective-permute-start | bytes 3932168 | tf_op jit(solution)/shard_map/ppermute | solution.py:30
  3.4 8.2 %copy-start.4 = (bf16[640,128]{1,0:T(8,128)(2,1)S(1)}, bf16[640,128]{1,0:T(8,128)(2,1)}, u32[]{:S(2)}) copy-start(bf16[640,128]{1,0:T(8,128)(2,1)} %get-tuple-element.31) | copy-start | bytes 491524
  3.4 32.1 %all-to-all-start = ((bf16[16,128,256]{2,1,0:T(8,128)(2,1)}), bf16[16,128,256]{2,1,0:T(8,128)(2,1)}, u32[]{:S(2)}, u32[]{:S(2)}) async-start(bf16[16,128,256]{2,1,0:T(8,128)(2,1)} %get-tuple-element.26), calls=%async_computation | async-start | bytes 2097152 | tf_op jit(solution)/shard_map/all_to_all | solution.py:373
  11.6 19.2 %collective-permute-start.5 = (bf16[640,128]{1,0:T(8,128)(2,1)S(1)}, bf16[640,128]{1,0:T(8,128)(2,1)S(1)}, u32[]{:S(2)}, u32[]{:S(2)}) collective-permute-start(bf16[640,128]{1,0:T(8,128)(2,1)S(1)} %copy-done.4), channel_id=1, source_target_pairs={{0,8},{8,16},{16,24},{24,0},{1,9},{9,17},{17,25},{25,1},{2,10},{10... | collective-permute-start | bytes 491528 | tf_op jit(solution)/shard_map/ppermute | solution.py:34
  13.5 20.3 %collective-permute-start.6 = (bf16[640,128]{1,0:T(8,128)(2,1)S(1)}, bf16[640,128]{1,0:T(8,128)(2,1)S(1)}, u32[]{:S(2)}, u32[]{:S(2)}) collective-permute-start(bf16[640,128]{1,0:T(8,128)(2,1)S(1)} %copy-done.4), channel_id=1, source_target_pairs={{0,16},{8,24},{16,0},{24,8},{1,17},{9,25},{17,1},{25,9},{2,18},{10... | collective-permute-start | bytes 491528 | tf_op jit(solution)/shard_map/ppermute | solution.py:34
  16.2 19.2 %collective-permute-start.4 = (bf16[640,128]{1,0:T(8,128)(2,1)S(1)}, bf16[640,128]{1,0:T(8,128)(2,1)S(1)}, u32[]{:S(2)}, u32[]{:S(2)}) collective-permute-start(bf16[640,128]{1,0:T(8,128)(2,1)S(1)} %copy-done.4), channel_id=1, source_target_pairs={{0,24},{8,0},{16,8},{24,16},{1,25},{9,1},{17,9},{25,17},{2,26},{10... | collective-permute-start | bytes 491528 | tf_op jit(solution)/shard_map/ppermute | solution.py:34
  33.9 38.4 %collective-permute-start.10 = (bf16[2,640,128]{2,1,0:T(8,128)(2,1)S(1)}, bf16[2,640,128]{2,1,0:T(8,128)(2,1)}, u32[]{:S(2)}, u32[]{:S(2)}) collective-permute-start(bf16[2,640,128]{2,1,0:T(8,128)(2,1)S(1)} %pad_maximum_fusion.2.old_0b), channel_id=1, source_target_pairs={{0,32},{32,64},{64,96},{96,0},{1,33},{33,65},{65,97},{97,1},{2,34}... | collective-permute-start | bytes 983048 | tf_op jit(solution)/shard_map/ppermute | solution.py:34
  35.4 60.2 %collective-permute-start.3 = (bf16[2048,256]{1,0:T(8,128)(2,1)}, bf16[2048,256]{1,0:T(8,128)(2,1)}, u32[]{:S(2)}, u32[]{:S(2)}) collective-permute-start(bf16[2048,256]{1,0:T(8,128)(2,1)} %bitcast.6.basis.basis_own), channel_id=1, source_target_pairs={{0,1},{1,0},{2,3},{3,2},{4,5},{5,4},{6,7},{7,6},{8,9},{9,8},{10,11... | collective-permute-start | bytes 3145736 | tf_op jit(solution)/shard_map/ppermute | solution.py:30
  49.0 37.1 %copy-start.2 = (bf16[128,256]{1,0:T(8,128)(2,1)S(1)}, bf16[128,256]{1,0:T(8,128)(2,1)}, u32[]{:S(2)}) copy-start(bf16[128,256]{1,0:T(8,128)(2,1)} %b_in.1) | copy-start | bytes 196612
  49.0 37.1 %copy-start.3 = (bf16[128,256]{1,0:T(8,128)(2,1)S(1)}, bf16[128,256]{1,0:T(8,128)(2,1)}, u32[]{:S(2)}) copy-start(bf16[128,256]{1,0:T(8,128)(2,1)} %b_out.1) | copy-start | bytes 196612
  49.0 14.9 %all-to-all-start.1 = ((bf16[16,16,640]{2,1,0:T(8,128)(2,1)}), bf16[16,16,640]{2,1,0:T(8,128)(2,1)S(1)}, u32[]{:S(2)}, u32[]{:S(2)}) async-start(bf16[16,16,640]{2,1,0:T(8,128)(2,1)} %bitcast.19), calls=%async_computation.1 | async-start | bytes 655360 | tf_op jit(solution)/shard_map/all_to_all | solution.py:396
  53.9 19.5 %collective-permute-start.7 = (bf16[2,640,128]{2,1,0:T(8,128)(2,1)S(1)}, bf16[2,640,128]{2,1,0:T(8,128)(2,1)S(1)}, u32[]{:S(2)}, u32[]{:S(2)}) collective-permute-start(bf16[2,640,128]{2,1,0:T(8,128)(2,1)S(1)} %pad_maximum_fusion.1.old_0a), channel_id=1, source_target_pairs={{0,96},{32,0},{64,32},{96,64},{1,97},{33,1},{65,33},{97,65},{2,98}... | collective-permute-start | bytes 983048 | tf_op jit(solution)/shard_map/ppermute | solution.py:34
  64.7 10.4 %collective-permute-start.2 = (f32[16,320]{1,0:T(8,128)S(1)}, f32[16,320]{1,0:T(8,128)S(1)}, u32[]{:S(2)}, u32[]{:S(2)}) collective-permute-start(f32[16,320]{1,0:T(8,128)S(1)} %get-tuple-element.29), channel_id=1, source_target_pairs={{0,1},{1,0},{2,3},{3,2},{4,5},{5,4},{6,7},{7,6},{8,9},{9,8},{10,11... | collective-permute-start | bytes 61448 | tf_op jit(solution)/shard_map/ppermute | solution.py:30
  64.7 30.9 %collective-permute-start.8 = (bf16[2,640,128]{2,1,0:T(8,128)(2,1)S(1)}, bf16[2,640,128]{2,1,0:T(8,128)(2,1)S(1)}, u32[]{:S(2)}, u32[]{:S(2)}) collective-permute-start(bf16[2,640,128]{2,1,0:T(8,128)(2,1)S(1)} %pad_maximum_fusion.2.old_0b), channel_id=1, source_target_pairs={{0,96},{32,0},{64,32},{96,64},{1,97},{33,1},{65,33},{97,65},{2,98}... | collective-permute-start | bytes 983048 | tf_op jit(solution)/shard_map/ppermute | solution.py:34
  65.6 15.9 %all-to-all-start.2 = ((f32[128,1,128]{2,1,0:T(1,128)}), f32[128,1,128]{2,1,0:T(1,128)S(1)}, u32[]{:S(2)}, u32[]{:S(2)}) async-start(f32[128,1,128]{2,1,0:T(1,128)} %get-tuple-element.27), calls=%async_computation.2 | async-start | bytes 131072 | tf_op jit(solution)/shard_map/all_to_all | solution.py:404
  72.2 23.4 %collective-permute-start.9 = (bf16[2,640,128]{2,1,0:T(8,128)(2,1)S(1)}, bf16[2,640,128]{2,1,0:T(8,128)(2,1)S(1)}, u32[]{:S(2)}, u32[]{:S(2)}) collective-permute-start(bf16[2,640,128]{2,1,0:T(8,128)(2,1)S(1)} %pad_maximum_fusion.1.old_0a), channel_id=1, source_target_pairs={{0,32},{32,64},{64,96},{96,0},{1,33},{33,65},{65,97},{97,1},{2,34}... | collective-permute-start | bytes 983048 | tf_op jit(solution)/shard_map/ppermute | solution.py:34
  73.4 22.2 %collective-permute-start.12 = (bf16[2,640,128]{2,1,0:T(8,128)(2,1)}, bf16[2,640,128]{2,1,0:T(8,128)(2,1)S(1)}, u32[]{:S(2)}, u32[]{:S(2)}) collective-permute-start(bf16[2,640,128]{2,1,0:T(8,128)(2,1)} %collective-permute-done.10.old_3b), channel_id=1, source_target_pairs={{0,32},{32,64},{64,96},{96,0},{1,33},{33,65},{65,97},{97,1},{2,34}... | collective-permute-start | bytes 983048 | tf_op jit(solution)/shard_map/ppermute | solution.py:34
  75.1 20.5 %collective-permute-start.11 = (bf16[2,640,128]{2,1,0:T(8,128)(2,1)S(1)}, bf16[2,640,128]{2,1,0:T(8,128)(2,1)S(1)}, u32[]{:S(2)}, u32[]{:S(2)}) collective-permute-start(bf16[2,640,128]{2,1,0:T(8,128)(2,1)S(1)} %collective-permute-done.7.old_1a), channel_id=1, source_target_pairs={{0,96},{32,0},{64,32},{96,64},{1,97},{33,1},{65,33},{97,65},{2,98}... | collective-permute-start | bytes 983048 | tf_op jit(solution)/shard_map/ppermute | solution.py:34
  82.5 13.1 %all-to-all-start.3 = ((bf16[16,16,640]{2,1,0:T(8,128)(2,1)}), bf16[16,16,640]{2,1,0:T(8,128)(2,1)S(1)}, u32[]{:S(2)}, u32[]{:S(2)}) async-start(bf16[16,16,640]{2,1,0:T(8,128)(2,1)} %get-tuple-element.30), calls=%async_computation.3 | async-start | bytes 655360 | tf_op jit(solution)/shard_map/all_to_all | solution.py:409

commit v3 on v2

--- a/solution.py
+++ b/solution.py
@@ -247,15 +247,14 @@
 
 
 def final_kernel(
-    core,
     at_x,
     at_z,
     full,
     mark,
     bases,
     weights,
-    basis_own,
-    basis_other,
+    whole_in,
+    whole_out,
     old_0a,
     old_0b,
     old_1a,
@@ -272,7 +271,6 @@
     copy_out,
     turned,
 ):
-    takes_in = core[0] == 0
     n = pl.program_id(0)
 
     @pl.when(n == 0)
@@ -285,12 +283,9 @@
         new_in[...] = weights[0:W] - 0.02 * own_in
         new_out[...] = weights[W:] - 0.02 * own_out
 
-    own = basis_own[...]
-    other = basis_other[...]
-
     def write(block_of):
-        s_in = contract(turned[0:W], jnp.where(takes_in, own, other), ((1,), (1,)))
-        s_out = contract(turned[W:], jnp.where(takes_in, other, own), ((1,), (1,)))
+        s_in = contract(turned[0:W], whole_in[...], ((1,), (1,)))
+        s_out = contract(turned[W:], whole_out[...], ((1,), (1,)))
         for k in range(SIDE):
             block = block_of(swap_last((k - at_x[0]) & (SIDE - 1))).astype(F32)
             cols = slice(128 * k, 128 * (k + 1))
@@ -305,7 +300,7 @@
             write(lambda r: jnp.where(r < 2, near[r & 1], far[r & 1]))
 
 
-def final(core, at_x, at_z, full, mark, bases, weights, own, other, old):
+def final(at_x, at_z, full, mark, bases, weights, whole_in, whole_out, old):
     shape = jax.ShapeDtypeStruct
 
     def whole(s):
@@ -315,12 +310,12 @@
         return (at_z[0] + swap_last(i)) & (SIDE - 1)
 
     tall = whole((W, 128))
-    tile = pl.BlockSpec((512, RANK), lambda i, core, at_x, at_z: (place(i, at_z), 0))
-    copy = pl.BlockSpec((W, 512), lambda i, core, at_x, at_z: (0, place(i, at_z)))
+    tile = pl.BlockSpec((512, RANK), lambda i, at_x, at_z: (place(i, at_z), 0))
+    copy = pl.BlockSpec((W, 512), lambda i, at_x, at_z: (0, place(i, at_z)))
     return pl.pallas_call(
         final_kernel,
         grid_spec=pltpu.PrefetchScalarGridSpec(
-            num_scalar_prefetch=3,
+            num_scalar_prefetch=2,
             grid=(SIDE,),
             in_specs=[
                 whole((RANK, 2 * W)),
@@ -347,7 +342,7 @@
         cost_estimate=pl.CostEstimate(
             flops=700_000_000, bytes_accessed=10_000_000, transcendentals=0
         ),
-    )(core, at_x, at_z, full, mark, bases, weights, own, other, *old)
+    )(at_x, at_z, full, mark, bases, weights, whole_in, whole_out, *old)
 
 
 def shards(
@@ -408,8 +403,14 @@
     )
     full = lax.all_to_all(dirs, FS, 0, 0, tiled=True).reshape(RANK, 2 * W)
     mark = lax.optimization_barrier(full[:8, :128])
+    sides = lax.optimization_barrier(
+        (
+            jnp.where(core[0] == 0, basis_own, basis_other),
+            jnp.where(core[0] == 0, basis_other, basis_own),
+        )
+    )
     step_in, new_in, copy_in, step_out, new_out, copy_out = final(
-        core, at_x, at_z, full, mark, own_bases, old_weights, basis_own, basis_other, old
+        at_x, at_z, full, mark, own_bases, old_weights, *sides, old
     )
     return (
         step_in.T,

time: 102 us -> 105 us (1.029)
  waiting for transfers between devices: 36.6 us -> 42.5 us
  Pallas kernels: 22.8 us -> 20.7 us
  starting transfers between devices: 39.9 us -> 38.3 us
    all_to_all x1, waiting for transfers between devices: 0.01 us -> 12.5 us  [shards(): basis_own = lax.all_to_all(bases, FS, 0, 0, tiled=True).reshape(-1, RANK)]
    all_to_all x1, waiting for transfers between devices: 9.49 us -> 3.02 us  [shards(): full = lax.all_to_all(dirs, FS, 0, 0, tiled=True).reshape(RANK, 2 * W)]
    all_to_all x1, waiting for transfers between devices: 4.06 us -> 9.2 us  [shards(): totals = lax.all_to_all(squares, EVERY, 0, 0, tiled=True)]
    ppermute x9, waiting for transfers between devices: 16.1 us -> 11.1 us  [shifted(): lax.ppermute(array, axis, [(i, (i + by) % SIDE) for i in range(SIDE)])]
    pallas_call x1, Pallas kernels: 5.44 us -> 3.41 us  [final(): pl.pallas_call(final_kernel, grid_spec=pltpu.PrefetchScalarGridSpec(num_s...]
    select_n x0 -> x1, other arithmetic: none -> 1.68 us  [shards(): jnp.where(core[0] == 0, basis_other, basis_own)]
    all_to_all x1, starting transfers between devices: 4.91 us -> 3.78 us  [shards(): lax.all_to_all(part.reshape(PEERS, ROWS, 2 * W), FS, split_axis=0, concat...]
  transfers between devices with their start and end apart: 17 -> 17, of which waited for: 5 -> 7; matrix products, arithmetic and copies ran while one was open for 1% -> 2% of each run, Pallas kernels for 17% -> 17%
where the time goes in v3:
time: 105 us; the launch traced here: 104 us
  waiting for transfers between devices  42.5 us (40%)
  starting transfers between devices  38.3 us (36%)
  Pallas kernels  20.7 us (20%)
  other arithmetic  1.81 us (2%)
    ppermute x9, starting transfers between devices, shifted(): lax.ppermute(array, axis, [(i, (i + by) % SIDE) for i in range(SIDE)])  15.9 us
    all_to_all x1, waiting for transfers between devices, shards(): basis_own = lax.all_to_all(bases, FS, 0, 0, tiled=True).reshape(-1, RANK)  12.5 us
    ppermute x9, waiting for transfers between devices, shifted(): lax.ppermute(array, axis, [(i, (i + by) % SIDE) for i in range(SIDE)])  11.1 us
    pallas_call x1, Pallas kernels, grad(): pl.pallas_call(grad_kernel, in_specs=[SMEM] + [pl.BlockSpec(memory_space=...  10 us
    all_to_all x1, waiting for transfers between devices, shards(): totals = lax.all_to_all(squares, EVERY, 0, 0, tiled=True)  9.2 us
    all_to_all x1, starting transfers between devices, shards(): basis_own = lax.all_to_all(bases, FS, 0, 0, tiled=True).reshape(-1, RANK)  8.17 us
    all_to_all x1, waiting for transfers between devices, shards(): lax.all_to_all(part.reshape(PEERS, ROWS, 2 * W), FS, split_axis=0, concat...  6.67 us
    all_to_all x1, starting transfers between devices, shards(): totals = lax.all_to_all(squares, EVERY, 0, 0, tiled=True)  6.34 us
  transfers between devices with their start and end apart: 17, of which 7 were waited for; matrix products, arithmetic and copies ran while one was open for 2% of the time, Pallas kernels for 17%

profile of v3, /device:TPU:0, one launch (start us, length us, event | category | flops | bytes accessed | tf_op | source)
XLA Modules:
  0.0 104.3 jit_solution(9523202422111998165)
XLA Ops:
  0.6 0.0 copy-start
  0.7 0.0 copy-start.1
  0.7 0.1 collective-permute-start
  0.8 0.5 collective-permute-start.1
  1.3 2.1 %pack.1 = (bf16[640,128]{1,0:T(8,128)(2,1)}, bf16[16,128,256]{2,1,0:T(8,128)(2,1)}) custom-call(s32[1]{0:T(128)} %bitcast.2.core, s32[1]{0:T(128)} %bitcast.at_x, s32[1]{0:T(128)} %bitcast.1.at_z, f32[320,128]{1,0:T(8,128)} %bitcast.26, f32[320,128]{1,0:T(8,128)} %w_out.1, bf16[128,256]{1,0:T(8,128)(2,1)} %b_in.1, bf16[128,256]{1,0:T(8,128)(2,1)} %b_out.1), custom_call_target="tpu_custom_call" | custom-call | flops 1000000 | bytes 500000 | tf_op jit(solution)/shard_map/pack/pallas_call | solution.py:50
  3.4 0.0 copy-start.8
  3.4 8.2 %all-to-all-start = ((bf16[16,128,256]{2,1,0:T(8,128)(2,1)}), bf16[16,128,256]{2,1,0:T(8,128)(2,1)}, u32[]{:S(2)}, u32[]{:S(2)}) async-start(bf16[16,128,256]{2,1,0:T(8,128)(2,1)} %get-tuple-element.28), calls=%async_computation | async-start | bytes 2097152 | tf_op jit(solution)/shard_map/all_to_all | solution.py:368
  11.6 0.0 copy-done.8
  11.6 1.9 %collective-permute-start.5 = (bf16[640,128]{1,0:T(8,128)(2,1)S(1)}, bf16[640,128]{1,0:T(8,128)(2,1)S(1)}, u32[]{:S(2)}, u32[]{:S(2)}) collective-permute-start(bf16[640,128]{1,0:T(8,128)(2,1)S(1)} %copy-done.8), channel_id=1, source_target_pairs={{0,8},{8,16},{16,24},{24,0},{1,9},{9,17},{17,25},{25,1},{2,10},{10... | collective-permute-start | bytes 491528 | tf_op jit(solution)/shard_map/ppermute | solution.py:34
  13.5 2.7 %collective-permute-start.6 = (bf16[640,128]{1,0:T(8,128)(2,1)S(1)}, bf16[640,128]{1,0:T(8,128)(2,1)S(1)}, u32[]{:S(2)}, u32[]{:S(2)}) collective-permute-start(bf16[640,128]{1,0:T(8,128)(2,1)S(1)} %copy-done.8), channel_id=1, source_target_pairs={{0,16},{8,24},{16,0},{24,8},{1,17},{9,25},{17,1},{25,9},{2,18},{10... | collective-permute-start | bytes 491528 | tf_op jit(solution)/shard_map/ppermute | solution.py:34
  16.2 1.5 %collective-permute-start.4 = (bf16[640,128]{1,0:T(8,128)(2,1)S(1)}, bf16[640,128]{1,0:T(8,128)(2,1)S(1)}, u32[]{:S(2)}, u32[]{:S(2)}) collective-permute-start(bf16[640,128]{1,0:T(8,128)(2,1)S(1)} %copy-done.8), channel_id=1, source_target_pairs={{0,24},{8,0},{16,8},{24,16},{1,25},{9,1},{17,9},{25,17},{2,26},{10... | collective-permute-start | bytes 491528 | tf_op jit(solution)/shard_map/ppermute | solution.py:34
  17.6 0.0 copy-done
  17.6 0.0 copy-done.1
  17.7 12.5 %all-to-all-done = bf16[16,128,256]{2,1,0:T(8,128)(2,1)} async-done(((bf16[16,128,256]{2,1,0:T(8,128)(2,1)}), bf16[16,128,256]{2,1,0:T(8,128)(2,1)}, u32[]{:S(2)}, u32[]{:S(2)}) %all-to-all-start) | async-done | bytes 1048608 | tf_op jit(solution)/shard_map/all_to_all | solution.py:368
  30.1 0.0 collective-permute-done.conv_came
  30.1 0.0 collective-permute-start.3
  30.1 0.0 collective-permute-done.1.lru_came
  30.1 10.0 %grad.1.grads = bf16[640,2048]{1,0:T(8,128)(2,1)} custom-call(s32[1]{0:T(128)} %bitcast.2.core, bf16[320,2048]{1,0:T(8,128)(2,1)} %bitcast.23, bf16[320,2048]{1,0:T(8,128)(2,1)} %collective-permute-done.conv_came, bf16[320,2048]{1,0:T(8,128)(2,1)} %bitcast.25, bf16[320,2048]{1,0:T(8,128)(2,1)} %collective-permute-done.1.lru_came, bf16[2048,2048]{1,0:T(8,128)(2,1)} %h.1, ...), custom_call_target="tpu_custom_call" | custom-call | flops 5368709120 | bytes 14000000 | tf_op jit(solution)/shard_map/grad/pallas_call | solution.py:113
  40.2 3.4 %project.1 = bf16[256,640]{1,0:T(8,128)(2,1)} custom-call(bf16[640,2048]{1,0:T(8,128)(2,1)} %grad.1.grads, bf16[2048,256]{1,0:T(8,128)(2,1)} %bitcast.6.basis), custom_call_target="tpu_custom_call" | custom-call | flops 671088640 | bytes 4000000 | tf_op jit(solution)/shard_map/project/pallas_call | solution.py:161
  43.5 0.0 copy-start.4
  43.6 0.0 copy-start.5
  43.6 0.0 copy-start.6
  43.6 0.0 copy-start.7
  43.6 3.8 %all-to-all-start.1 = ((bf16[16,16,640]{2,1,0:T(8,128)(2,1)}), bf16[16,16,640]{2,1,0:T(8,128)(2,1)S(1)}, u32[]{:S(2)}, u32[]{:S(2)}) async-start(bf16[16,16,640]{2,1,0:T(8,128)(2,1)} %bitcast.21), calls=%async_computation.1 | async-start | bytes 655360 | tf_op jit(solution)/shard_map/all_to_all | solution.py:391
  47.4 0.0 collective-permute-done.5
  47.4 0.0 collective-permute-done.6
  47.4 0.0 copy-start.2
  47.4 0.0 copy-start.3
  47.5 2.0 %collective-permute-start.10 = (bf16[2,640,128]{2,1,0:T(8,128)(2,1)S(1)}, bf16[2,640,128]{2,1,0:T(8,128)(2,1)S(1)}, u32[]{:S(2)}, u32[]{:S(2)}) collective-permute-start(bf16[2,640,128]{2,1,0:T(8,128)(2,1)S(1)} %pad_maximum_fusion.2.old_0b), channel_id=1, source_target_pairs={{0,32},{32,64},{64,96},{96,0},{1,33},{33,65},{65,97},{97,1},{2,34}... | collective-permute-start | bytes 983048 | tf_op jit(solution)/shard_map/ppermute | solution.py:34
  49.5 0.0 collective-permute-done.4
  49.5 1.4 %collective-permute-start.7 = (bf16[2,640,128]{2,1,0:T(8,128)(2,1)S(1)}, bf16[2,640,128]{2,1,0:T(8,128)(2,1)S(1)}, u32[]{:S(2)}, u32[]{:S(2)}) collective-permute-start(bf16[2,640,128]{2,1,0:T(8,128)(2,1)S(1)} %pad_maximum_fusion.1.old_0a), channel_id=1, source_target_pairs={{0,96},{32,0},{64,32},{96,64},{1,97},{33,1},{65,33},{97,65},{2,98}... | collective-permute-start | bytes 983048 | tf_op jit(solution)/shard_map/ppermute | solution.py:34
  50.9 6.7 %all-to-all-done.1.arrived = bf16[16,16,640]{2,1,0:T(8,128)(2,1)S(1)} async-done(((bf16[16,16,640]{2,1,0:T(8,128)(2,1)}), bf16[16,16,640]{2,1,0:T(8,128)(2,1)S(1)}, u32[]{:S(2)}, u32[]{:S(2)}) %all-to-all-start.1) | async-done | bytes 327712 | tf_op jit(solution)/shard_map/all_to_all | solution.py:391
  57.6 0.8 collect.1
  58.4 0.0 collective-permute-start.2
  58.4 6.3 %all-to-all-start.2 = ((f32[128,1,128]{2,1,0:T(1,128)}), f32[128,1,128]{2,1,0:T(1,128)S(1)}, u32[]{:S(2)}, u32[]{:S(2)}) async-start(f32[128,1,128]{2,1,0:T(1,128)} %get-tuple-element.29), calls=%async_computation.2 | async-start | bytes 131072 | tf_op jit(solution)/shard_map/all_to_all | solution.py:399
  64.7 0.0 copy-done.4
  64.7 0.0 copy-done.5
  64.7 0.0 copy-done.6
  64.8 0.0 copy-done.7
  64.8 0.0 collective-permute-done.2.came
  64.8 9.2 %all-to-all-done.2.totals = f32[128,1,128]{2,1,0:T(1,128)S(1)} async-done(((f32[128,1,128]{2,1,0:T(1,128)}), f32[128,1,128]{2,1,0:T(1,128)S(1)}, u32[]{:S(2)}, u32[]{:S(2)}) %all-to-all-start.2) | async-done | bytes 65568 | tf_op jit(solution)/shard_map/all_to_all | solution.py:399
  74.0 1.0 apply.1
  75.0 3.5 %all-to-all-start.3 = ((bf16[16,16,640]{2,1,0:T(8,128)(2,1)}), bf16[16,16,640]{2,1,0:T(8,128)(2,1)S(1)}, u32[]{:S(2)}, u32[]{:S(2)}) async-start(bf16[16,16,640]{2,1,0:T(8,128)(2,1)} %get-tuple-element.32), calls=%async_computation.3 | async-start | bytes 655360 | tf_op jit(solution)/shard_map/all_to_all | solution.py:404
  78.6 0.0 copy-done.2
  78.6 0.0 copy-done.3
  78.6 3.2 %collective-permute-start.8 = (bf16[2,640,128]{2,1,0:T(8,128)(2,1)S(1)}, bf16[2,640,128]{2,1,0:T(8,128)(2,1)S(1)}, u32[]{:S(2)}, u32[]{:S(2)}) collective-permute-start(bf16[2,640,128]{2,1,0:T(8,128)(2,1)S(1)} %pad_maximum_fusion.2.old_0b), channel_id=1, source_target_pairs={{0,96},{32,0},{64,32},{96,64},{1,97},{33,1},{65,33},{97,65},{2,98}... | collective-permute-start | bytes 983048 | tf_op jit(solution)/shard_map/ppermute | solution.py:34
  81.8 0.0 collective-permute-start.9
  81.8 0.0 collective-permute-done.10.old_3b
  81.8 0.8 collective-permute-start.12
  82.5 0.0 collective-permute-done.7.old_1a
  82.5 2.5 %collective-permute-start.11 = (bf16[2,640,128]{2,1,0:T(8,128)(2,1)S(1)}, bf16[2,640,128]{2,1,0:T(8,128)(2,1)S(1)}, u32[]{:S(2)}, u32[]{:S(2)}) collective-permute-start(bf16[2,640,128]{2,1,0:T(8,128)(2,1)S(1)} %collective-permute-done.7.old_1a), channel_id=1, source_target_pairs={{0,96},{32,0},{64,32},{96,64},{1,97},{33,1},{65,33},{97,65},{2,98}... | collective-permute-start | bytes 983048 | tf_op jit(solution)/shard_map/ppermute | solution.py:34
  85.1 3.0 %all-to-all-done.3 = bf16[16,16,640]{2,1,0:T(8,128)(2,1)S(1)} async-done(((bf16[16,16,640]{2,1,0:T(8,128)(2,1)}), bf16[16,16,640]{2,1,0:T(8,128)(2,1)S(1)}, u32[]{:S(2)}, u32[]{:S(2)}) %all-to-all-start.3) | async-done | bytes 327712 | tf_op jit(solution)/shard_map/all_to_all | solution.py:404
  88.1 0.0 collective-permute-done.3
  88.1 1.7 %broadcast_select_fusion = (bf16[2048,256]{1,0:T(8,128)(2,1)S(1)}, bf16[2048,256]{1,0:T(8,128)(2,1)S(1)}) fusion(bf16[2048,256]{1,0:T(8,128)(2,1)} %collective-permute-done.3, pred[]{:T(512)S(6)} %eq.4, bf16[16,128,256]{2,1,0:T(8,128)(2,1)} %all-to-all-done), kind=kLoop, calls=%fused_computation | loop fusion | flops 1048576 | bytes 4194305 | tf_op jit(solution)/shard_map/jit(_where)/select_n | solution.py:409
  89.8 2.9 %collective-permute-done.8.old_1b = bf16[2,640,128]{2,1,0:T(8,128)(2,1)S(1)} collective-permute-done((bf16[2,640,128]{2,1,0:T(8,128)(2,1)S(1)}, bf16[2,640,128]{2,1,0:T(8,128)(2,1)S(1)}, u32[]{:S(2)}, u32[]{:S(2)}) %collective-permute-start.8) | collective-permute-done | bytes 327712 | tf_op jit(solution)/shard_map/ppermute | solution.py:34
  92.7 1.6 %collective-permute-done.9.old_3a = bf16[2,640,128]{2,1,0:T(8,128)(2,1)S(1)} collective-permute-done((bf16[2,640,128]{2,1,0:T(8,128)(2,1)S(1)}, bf16[2,640,128]{2,1,0:T(8,128)(2,1)S(1)}, u32[]{:S(2)}, u32[]{:S(2)}) %collective-permute-start.9) | collective-permute-done | bytes 327712 | tf_op jit(solution)/shard_map/ppermute | solution.py:34
  94.3 6.6 %collective-permute-done.12.old_2b = bf16[2,640,128]{2,1,0:T(8,128)(2,1)S(1)} collective-permute-done((bf16[2,640,128]{2,1,0:T(8,128)(2,1)S(1)}, bf16[2,640,128]{2,1,0:T(8,128)(2,1)S(1)}, u32[]{:S(2)}, u32[]{:S(2)}) %collective-permute-start.12) | collective-permute-done | bytes 327712 | tf_op jit(solution)/shard_map/ppermute | solution.py:34
  100.9 0.0 collective-permute-done.11.old_2a
  100.9 3.4 %final.1 = (f32[320,128]{1,0:T(8,128)}, f32[320,128]{1,0:T(8,128)}, bf16[320,2048]{1,0:T(8,128)(2,1)}, f32[320,128]{1,0:T(8,128)}, f32[320,128]{1,0:T(8,128)}, /*index=5*/bf16[320,2048]{1,0:T(8,128)(2,1)}) custom-call(s32[1]{0:T(128)} %bitcast.at_x, s32[1]{0:T(128)} %bitcast.1.at_z, bf16[256,640]{1,0:T(8,128)(2,1)S(1)} %bitcast.20, ...), custom_call_target="tpu_custom_call" | custom-call | flops 700000000 | bytes 10000000 | tf_op jit(solution)/shard_map/final/pallas_call | solution.py:315
  (7 shorter events, 0.1 us)
Async XLA Ops:
  0.6 17.0 %copy-start = (f32[128,320]{0,1:T(8,128)S(1)}, f32[128,320]{0,1:T(8,128)}, u32[]{:S(2)}) copy-start(f32[128,320]{0,1:T(8,128)} %param.18) | copy-start | bytes 491524
  0.7 17.0 %copy-start.1 = (f32[320,128]{1,0:T(8,128)S(1)}, f32[320,128]{1,0:T(8,128)}, u32[]{:S(2)}) copy-start(f32[320,128]{1,0:T(8,128)} %w_out.1) | copy-start | bytes 491524
  0.7 29.5 %collective-permute-start = (bf16[320,2048]{1,0:T(8,128)(2,1)}, bf16[320,2048]{1,0:T(8,128)(2,1)}, u32[]{:S(2)}, u32[]{:S(2)}) collective-permute-start(bf16[320,2048]{1,0:T(8,128)(2,1)} %bitcast.22), channel_id=1, source_target_pairs={{0,1},{1,0},{2,3},{3,2},{4,5},{5,4},{6,7},{7,6},{8,9},{9,8},{10,11... | collective-permute-start | bytes 3932168 | tf_op jit(solution)/shard_map/ppermute | solution.py:30
  0.8 29.4 %collective-permute-start.1 = (bf16[320,2048]{1,0:T(8,128)(2,1)}, bf16[320,2048]{1,0:T(8,128)(2,1)}, u32[]{:S(2)}, u32[]{:S(2)}) collective-permute-start(bf16[320,2048]{1,0:T(8,128)(2,1)} %bitcast.24), channel_id=1, source_target_pairs={{0,1},{1,0},{2,3},{3,2},{4,5},{5,4},{6,7},{7,6},{8,9},{9,8},{10,11... | collective-permute-start | bytes 3932168 | tf_op jit(solution)/shard_map/ppermute | solution.py:30
  3.4 8.2 %copy-start.8 = (bf16[640,128]{1,0:T(8,128)(2,1)S(1)}, bf16[640,128]{1,0:T(8,128)(2,1)}, u32[]{:S(2)}) copy-start(bf16[640,128]{1,0:T(8,128)(2,1)} %get-tuple-element.35) | copy-start | bytes 491524
  3.4 26.8 %all-to-all-start = ((bf16[16,128,256]{2,1,0:T(8,128)(2,1)}), bf16[16,128,256]{2,1,0:T(8,128)(2,1)}, u32[]{:S(2)}, u32[]{:S(2)}) async-start(bf16[16,128,256]{2,1,0:T(8,128)(2,1)} %get-tuple-element.28), calls=%async_computation | async-start | bytes 2097152 | tf_op jit(solution)/shard_map/all_to_all | solution.py:368
  11.6 35.8 %collective-permute-start.5 = (bf16[640,128]{1,0:T(8,128)(2,1)S(1)}, bf16[640,128]{1,0:T(8,128)(2,1)S(1)}, u32[]{:S(2)}, u32[]{:S(2)}) collective-permute-start(bf16[640,128]{1,0:T(8,128)(2,1)S(1)} %copy-done.8), channel_id=1, source_target_pairs={{0,8},{8,16},{16,24},{24,0},{1,9},{9,17},{17,25},{25,1},{2,10},{10... | collective-permute-start | bytes 491528 | tf_op jit(solution)/shard_map/ppermute | solution.py:34
  13.5 33.9 %collective-permute-start.6 = (bf16[640,128]{1,0:T(8,128)(2,1)S(1)}, bf16[640,128]{1,0:T(8,128)(2,1)S(1)}, u32[]{:S(2)}, u32[]{:S(2)}) collective-permute-start(bf16[640,128]{1,0:T(8,128)(2,1)S(1)} %copy-done.8), channel_id=1, source_target_pairs={{0,16},{8,24},{16,0},{24,8},{1,17},{9,25},{17,1},{25,9},{2,18},{10... | collective-permute-start | bytes 491528 | tf_op jit(solution)/shard_map/ppermute | solution.py:34
  16.2 33.3 %collective-permute-start.4 = (bf16[640,128]{1,0:T(8,128)(2,1)S(1)}, bf16[640,128]{1,0:T(8,128)(2,1)S(1)}, u32[]{:S(2)}, u32[]{:S(2)}) collective-permute-start(bf16[640,128]{1,0:T(8,128)(2,1)S(1)} %copy-done.8), channel_id=1, source_target_pairs={{0,24},{8,0},{16,8},{24,16},{1,25},{9,1},{17,9},{25,17},{2,26},{10... | collective-permute-start | bytes 491528 | tf_op jit(solution)/shard_map/ppermute | solution.py:34
  30.1 58.0 %collective-permute-start.3 = (bf16[2048,256]{1,0:T(8,128)(2,1)}, bf16[2048,256]{1,0:T(8,128)(2,1)}, u32[]{:S(2)}, u32[]{:S(2)}) collective-permute-start(bf16[2048,256]{1,0:T(8,128)(2,1)} %bitcast.6.basis), channel_id=1, source_target_pairs={{0,1},{1,0},{2,3},{3,2},{4,5},{5,4},{6,7},{7,6},{8,9},{9,8},{10,11... | collective-permute-start | bytes 3145736 | tf_op jit(solution)/shard_map/ppermute | solution.py:30
  43.5 21.2 %copy-start.4 = (f32[16,320]{1,0:T(8,128)S(1)}, f32[16,320]{1,0:T(8,128)}, u32[]{:S(2)}) copy-start(f32[16,320]{1,0:T(8,128)} %param.23) | copy-start | bytes 61444
  43.6 21.2 %copy-start.5 = (f32[16,320]{1,0:T(8,128)S(1)}, f32[16,320]{1,0:T(8,128)}, u32[]{:S(2)}) copy-start(f32[16,320]{1,0:T(8,128)} %param.22) | copy-start | bytes 61444
  43.6 21.2 %copy-start.6 = (f32[16,320]{1,0:T(8,128)S(1)}, f32[16,320]{1,0:T(8,128)}, u32[]{:S(2)}) copy-start(f32[16,320]{1,0:T(8,128)} %param.21) | copy-start | bytes 61444
  43.6 21.2 %copy-start.7 = (f32[16,320]{1,0:T(8,128)S(1)}, f32[16,320]{1,0:T(8,128)}, u32[]{:S(2)}) copy-start(f32[16,320]{1,0:T(8,128)} %param.20) | copy-start | bytes 61444
  43.6 14.0 %all-to-all-start.1 = ((bf16[16,16,640]{2,1,0:T(8,128)(2,1)}), bf16[16,16,640]{2,1,0:T(8,128)(2,1)S(1)}, u32[]{:S(2)}, u32[]{:S(2)}) async-start(bf16[16,16,640]{2,1,0:T(8,128)(2,1)} %bitcast.21), calls=%async_computation.1 | async-start | bytes 655360 | tf_op jit(solution)/shard_map/all_to_all | solution.py:391
  47.4 31.1 %copy-start.2 = (bf16[128,256]{1,0:T(8,128)(2,1)S(1)}, bf16[128,256]{1,0:T(8,128)(2,1)}, u32[]{:S(2)}) copy-start(bf16[128,256]{1,0:T(8,128)(2,1)} %b_in.1) | copy-start | bytes 196612
  47.4 31.1 %copy-start.3 = (bf16[128,256]{1,0:T(8,128)(2,1)S(1)}, bf16[128,256]{1,0:T(8,128)(2,1)}, u32[]{:S(2)}) copy-start(bf16[128,256]{1,0:T(8,128)(2,1)} %b_out.1) | copy-start | bytes 196612
  47.5 34.3 %collective-permute-start.10 = (bf16[2,640,128]{2,1,0:T(8,128)(2,1)S(1)}, bf16[2,640,128]{2,1,0:T(8,128)(2,1)S(1)}, u32[]{:S(2)}, u32[]{:S(2)}) collective-permute-start(bf16[2,640,128]{2,1,0:T(8,128)(2,1)S(1)} %pad_maximum_fusion.2.old_0b), channel_id=1, source_target_pairs={{0,32},{32,64},{64,96},{96,0},{1,33},{33,65},{65,97},{97,1},{2,34}... | collective-permute-start | bytes 983048 | tf_op jit(solution)/shard_map/ppermute | solution.py:34
  49.5 33.0 %collective-permute-start.7 = (bf16[2,640,128]{2,1,0:T(8,128)(2,1)S(1)}, bf16[2,640,128]{2,1,0:T(8,128)(2,1)S(1)}, u32[]{:S(2)}, u32[]{:S(2)}) collective-permute-start(bf16[2,640,128]{2,1,0:T(8,128)(2,1)S(1)} %pad_maximum_fusion.1.old_0a), channel_id=1, source_target_pairs={{0,96},{32,0},{64,32},{96,64},{1,97},{33,1},{65,33},{97,65},{2,98}... | collective-permute-start | bytes 983048 | tf_op jit(solution)/shard_map/ppermute | solution.py:34
  58.4 6.4 %collective-permute-start.2 = (f32[16,320]{1,0:T(8,128)S(1)}, f32[16,320]{1,0:T(8,128)S(1)}, u32[]{:S(2)}, u32[]{:S(2)}) collective-permute-start(f32[16,320]{1,0:T(8,128)S(1)} %get-tuple-element.31), channel_id=1, source_target_pairs={{0,1},{1,0},{2,3},{3,2},{4,5},{5,4},{6,7},{7,6},{8,9},{9,8},{10,11... | collective-permute-start | bytes 61448 | tf_op jit(solution)/shard_map/ppermute | solution.py:30
  58.4 15.6 %all-to-all-start.2 = ((f32[128,1,128]{2,1,0:T(1,128)}), f32[128,1,128]{2,1,0:T(1,128)S(1)}, u32[]{:S(2)}, u32[]{:S(2)}) async-start(f32[128,1,128]{2,1,0:T(1,128)} %get-tuple-element.29), calls=%async_computation.2 | async-start | bytes 131072 | tf_op jit(solution)/shard_map/all_to_all | solution.py:399
  75.0 13.1 %all-to-all-start.3 = ((bf16[16,16,640]{2,1,0:T(8,128)(2,1)}), bf16[16,16,640]{2,1,0:T(8,128)(2,1)S(1)}, u32[]{:S(2)}, u32[]{:S(2)}) async-start(bf16[16,16,640]{2,1,0:T(8,128)(2,1)} %get-tuple-element.32), calls=%async_computation.3 | async-start | bytes 655360 | tf_op jit(solution)/shard_map/all_to_all | solution.py:404
  78.6 14.1 %collective-permute-start.8 = (bf16[2,640,128]{2,1,0:T(8,128)(2,1)S(1)}, bf16[2,640,128]{2,1,0:T(8,128)(2,1)S(1)}, u32[]{:S(2)}, u32[]{:S(2)}) collective-permute-start(bf16[2,640,128]{2,1,0:T(8,128)(2,1)S(1)} %pad_maximum_fusion.2.old_0b), channel_id=1, source_target_pairs={{0,96},{32,0},{64,32},{96,64},{1,97},{33,1},{65,33},{97,65},{2,98}... | collective-permute-start | bytes 983048 | tf_op jit(solution)/shard_map/ppermute | solution.py:34
  81.8 12.5 %collective-permute-start.9 = (bf16[2,640,128]{2,1,0:T(8,128)(2,1)S(1)}, bf16[2,640,128]{2,1,0:T(8,128)(2,1)S(1)}, u32[]{:S(2)}, u32[]{:S(2)}) collective-permute-start(bf16[2,640,128]{2,1,0:T(8,128)(2,1)S(1)} %pad_maximum_fusion.1.old_0a), channel_id=1, source_target_pairs={{0,32},{32,64},{64,96},{96,0},{1,33},{33,65},{65,97},{97,1},{2,34}... | collective-permute-start | bytes 983048 | tf_op jit(solution)/shard_map/ppermute | solution.py:34
  81.8 19.1 %collective-permute-start.12 = (bf16[2,640,128]{2,1,0:T(8,128)(2,1)S(1)}, bf16[2,640,128]{2,1,0:T(8,128)(2,1)S(1)}, u32[]{:S(2)}, u32[]{:S(2)}) collective-permute-start(bf16[2,640,128]{2,1,0:T(8,128)(2,1)S(1)} %collective-permute-done.10.old_3b), channel_id=1, source_target_pairs={{0,32},{32,64},{64,96},{96,0},{1,33},{33,65},{65,97},{97,1},{2,34}... | collective-permute-start | bytes 983048 | tf_op jit(solution)/shard_map/ppermute | solution.py:34
  82.5 18.4 %collective-permute-start.11 = (bf16[2,640,128]{2,1,0:T(8,128)(2,1)S(1)}, bf16[2,640,128]{2,1,0:T(8,128)(2,1)S(1)}, u32[]{:S(2)}, u32[]{:S(2)}) collective-permute-start(bf16[2,640,128]{2,1,0:T(8,128)(2,1)S(1)} %collective-permute-done.7.old_1a), channel_id=1, source_target_pairs={{0,96},{32,0},{64,32},{96,64},{1,97},{33,1},{65,33},{97,65},{2,98}... | collective-permute-start | bytes 983048 | tf_op jit(solution)/shard_map/ppermute | solution.py:34
